TPU v7x, 128 devices: a whole 4x4x4 slice. The times are simulated.
128 devices in a mesh: ep: 16 (over z, x), tp: 8 (over y, core).
Axes of the slice: x: 4, y: 4, z: 4, core: 2. Of those that a mesh axis runs over, the one named last changes fastest.
Arguments:
- residual: bfloat16 [1024, 4096], P('ep', 'tp'), may hold values from -64 to 64
- routes: int32 [1024, 2], P('ep'), may hold values from 0 to 15, all different within a row; in each aligned block of 64 rows (0 to 63, 64 to 127, ...) at most 16 rows name the same one
- route_weights: float32 [1024, 2], P('ep'), may hold values from 0.2 to 1
- state_prev: float32 [1024, 2, 64, 64], P('ep', None, 'tp'), may hold values from -6 to 6
- mix_gain: float32 [4096], replicated, may hold values from 0.1 to 1.9
- ffn_gain: float32 [4096], replicated, may hold values from 0.1 to 1.9
- w_in: bfloat16 [4096, 1024], P(None, 'tp'), may hold values from -0.09375 to 0.09375
- decay_rate: float32 [64, 64], P('tp'), may hold values from 0.5 to 8
- rotation: float32 [64, 64], P('tp'), may hold values from 0 to 200
- log_step: float32 [64], P('tp'), may hold values from -3.9 to -1.2
- in_re: float32 [64, 64, 16], P('tp'), may hold values from -1 to 1
- in_im: float32 [64, 64, 16], P('tp'), may hold values from -1 to 1
- read_re: float32 [64, 16, 64], P('tp'), may hold values from -0.5 to 0.5
- read_im: float32 [64, 16, 64], P('tp'), may hold values from -0.5 to 0.5
- skip_gain: float32 [64, 16], P('tp'), may hold values from -4 to 4
- w_glu: bfloat16 [1024, 1024], P(None, 'tp'), may hold values from -0.1875 to 0.1875
- w_out: bfloat16 [1024, 4096], P('tp'), may hold values from -0.1875 to 0.1875
- w_gate: bfloat16 [16, 4096, 5632], P('ep', None, 'tp'), may hold values from -0.09375 to 0.09375
- w_up: bfloat16 [16, 4096, 5632], P('ep', None, 'tp'), may hold values from -0.09375 to 0.09375
- w_down: bfloat16 [16, 5632, 4096], P('ep', 'tp'), may hold values from -0.078125 to 0.078125
Outputs:
- layer_out: bfloat16 [1024, 4096], P('ep', 'tp')
- state_next: float32 [1024, 2, 64, 64], P('ep', None, 'tp')
Inputs may be any that keep to these rules, and one draw needn't show every extreme that they name: `routes`: each row names 2 different experts. In each aligned block of 64 rows (the rows of one index of ep) no expert is named more than 16 times, a bound that some block reaches.
All inputs are finite; a program needn't handle non-finite values.
Results may differ from a plain program's by a relative error of at most 0.012.
Values may be sent and summed in bfloat16 or wider, within the bound.
A program may use at most 64 MiB of HBM per device.

v0:
```python
import jax
import jax.numpy as jnp
from jax import lax
from jax.sharding import PartitionSpec as P

GROUP_CH = 16
TOPK = 2


epsilon = 1e-06


def copy_for_each(array, axis):
    size = lax.axis_size(axis)
    return lax.all_to_all(
        jnp.broadcast_to(array[None], (size, *array.shape)), axis, 0, 0, tiled=True
    )


def laid_out(blocks, dim):
    blocks = jnp.moveaxis(blocks, 0, dim)
    dims = blocks.shape
    return blocks.reshape(*dims[:dim], dims[dim] * dims[dim + 1], *dims[dim + 2 :])


def gather_directly(array, axis, dim):
    blocks = copy_for_each(array, axis)
    return laid_out(blocks, dim)


def split_up(array, dim, size):
    before, after = (array.shape[:dim], array.shape[dim + 1 :])
    return jnp.moveaxis(array.reshape(*before, size, -1, *after), dim, 0)


def sent_and_summed(array, axis, dim):
    blocks = split_up(array, dim, lax.axis_size(axis))
    arrived = lax.all_to_all(blocks, axis, split_axis=0, concat_axis=0, tiled=True)
    return arrived.astype(jnp.float32).sum(axis=0)


def over_copies(array, axis):
    everything = copy_for_each(array, axis)
    return jnp.sum(everything, axis=0)


def state_mixer(
    u_in, state_prev, decay_rate, rotation, log_step, in_re, in_im, read_re, read_im, skip_gain
):
    batch_rows = u_in.shape[0]
    groups = decay_rate.shape[0]
    grouped = u_in.astype(jnp.float32).reshape(batch_rows, groups, GROUP_CH)
    step_size = jnp.exp(log_step)[:, None]
    real_part = -decay_rate
    magnitude = jnp.exp(real_part * step_size)
    decay_re = magnitude * jnp.cos(rotation * step_size)
    decay_im = magnitude * jnp.sin(rotation * step_size)
    denominator = real_part * real_part + rotation * rotation
    lift_re = ((decay_re - 1.0) * real_part + decay_im * rotation) / denominator
    lift_im = (decay_im * real_part - (decay_re - 1.0) * rotation) / denominator
    map_re = lift_re[..., None] * in_re - lift_im[..., None] * in_im
    map_im = lift_re[..., None] * in_im + lift_im[..., None] * in_re
    drive_re = jnp.einsum("gph,bgh->bgp", map_re, grouped)
    drive_im = jnp.einsum("gph,bgh->bgp", map_im, grouped)
    old_re = state_prev[:, 0]
    old_im = state_prev[:, 1]
    new_re = decay_re * old_re - decay_im * old_im + drive_re
    new_im = decay_re * old_im + decay_im * old_re + drive_im
    output = (
        jnp.einsum("ghp,bgp->bgh", read_re, new_re)
        - jnp.einsum("ghp,bgp->bgh", read_im, new_im)
        + skip_gain * grouped
    )
    return (jax.nn.gelu(output.reshape(batch_rows, -1)), jnp.stack([new_re, new_im], axis=1))


def per_device(
    residual,
    routes,
    route_weights,
    state_prev,
    mix_gain,
    ffn_gain,
    w_in,
    decay_rate,
    rotation,
    log_step,
    in_re,
    in_im,
    read_re,
    read_im,
    skip_gain,
    w_glu,
    w_out,
    w_gate,
    w_up,
    w_down,
):
    shard_width = residual.shape[1]
    full_width = shard_width * lax.axis_size("tp")
    tp_place = lax.axis_index("tp")
    experts_all = lax.axis_size("ep")
    seq_rows = residual.shape[0]
    capacity = 2 * seq_rows * TOPK // experts_all
    source = residual.astype(jnp.float32)
    gathered = gather_directly(residual, "tp", 1)
    whole_rows = gathered.astype(jnp.float32)
    scale_whole = lax.rsqrt(jnp.mean(whole_rows * whole_rows, axis=1, keepdims=True) + epsilon)
    normed_mix = (whole_rows * scale_whole * mix_gain).astype(jnp.bfloat16)
    u_in = jnp.dot(normed_mix, w_in, preferred_element_type=jnp.float32).astype(jnp.bfloat16)
    mixer_act, state_next = state_mixer(
        u_in, state_prev, decay_rate, rotation, log_step, in_re, in_im, read_re, read_im, skip_gain
    )
    mixer_bf = mixer_act.astype(jnp.bfloat16)
    all_channels = gather_directly(mixer_bf, "tp", 1)
    glu_logit = jnp.dot(all_channels, w_glu, preferred_element_type=jnp.float32)
    mixed = (mixer_act * jax.nn.sigmoid(glu_logit)).astype(jnp.bfloat16)
    partial_out = jnp.dot(mixed, w_out, preferred_element_type=jnp.float32)
    branch = sent_and_summed(partial_out.astype(jnp.bfloat16), "tp", 1)
    after_float = (source + branch).astype(jnp.bfloat16).astype(jnp.float32)
    squares_ffn = over_copies(jnp.sum(after_float * after_float, axis=1), "tp")
    ffn_own = lax.dynamic_slice_in_dim(ffn_gain, tp_place * shard_width, shard_width)
    scale_ffn = lax.rsqrt(squares_ffn / full_width + epsilon)[:, None]
    normed_ffn = (after_float * scale_ffn * ffn_own).astype(jnp.bfloat16)
    flat_routes = routes.reshape(-1)
    onehot = (flat_routes[:, None] == jnp.arange(experts_all, dtype=jnp.int32)).astype(jnp.int32)
    before = jnp.cumsum(onehot, axis=0) - onehot
    slot_index = jnp.sum(before * onehot, axis=1)
    destination = (flat_routes * capacity + slot_index).reshape(seq_rows, TOPK)
    matches = destination[:, :, None] == jnp.arange(experts_all * capacity, dtype=jnp.int32)
    dispatch_map = jnp.sum(matches.astype(jnp.float32), axis=1).astype(jnp.bfloat16)
    combine_map = jnp.sum(jnp.where(matches, route_weights[:, :, None], 0.0), axis=1)
    outbound = jnp.einsum("bj,bd->jd", dispatch_map, normed_ffn, preferred_element_type=jnp.float32)
    outbound = outbound.astype(jnp.bfloat16).reshape(experts_all, capacity, shard_width)
    arrived = gather_directly(
        lax.all_to_all(outbound, "ep", split_axis=0, concat_axis=0, tiled=True), "tp", 2
    )
    sources, slots_here, row_width = arrived.shape
    flat_rows = arrived.reshape(sources * slots_here, row_width)
    gate_value = jnp.dot(flat_rows, w_gate[0], preferred_element_type=jnp.float32)
    up_value = jnp.dot(flat_rows, w_up[0], preferred_element_type=jnp.float32)
    hidden = (jax.nn.silu(gate_value) * up_value).astype(jnp.bfloat16)
    partial_sum = jnp.dot(hidden, w_down[0], preferred_element_type=jnp.float32)
    partial_sum = partial_sum.reshape(sources, slots_here, row_width)
    reduced = sent_and_summed(partial_sum.astype(jnp.bfloat16), "tp", 2)
    expert_out = reduced.astype(jnp.bfloat16)
    came_back = lax.all_to_all(expert_out, "ep", split_axis=0, concat_axis=0, tiled=True)
    came_back = came_back.reshape(experts_all * capacity, shard_width).astype(jnp.float32)
    combined = jnp.dot(combine_map, came_back)
    layer_out = (after_float + combined).astype(jnp.bfloat16)
    return (layer_out, state_next)


def solution(mesh):
    return jax.shard_map(
        per_device,
        mesh=mesh,
        in_specs=(
            P("ep", "tp"),
            P("ep", None),
            P("ep", None),
            P("ep", None, "tp", None),
            P(),
            P(),
            P(None, "tp"),
            P("tp", None),
            P("tp", None),
            P("tp"),
            P("tp", None, None),
            P("tp", None, None),
            P("tp", None, None),
            P("tp", None, None),
            P("tp", None),
            P(None, "tp"),
            P("tp", None),
            P("ep", None, "tp"),
            P("ep", None, "tp"),
            P("ep", "tp", None),
        ),
        out_specs=(P("ep", "tp"), P("ep", None, "tp", None)),
        check_vma=False,
    )
```

profile of v0, /device:TPU:0, one launch (start us, length us, event | category | flops | bytes accessed | tf_op | source)
XLA Modules:
  0.0 155.8 jit_solution(4993328798136662543)
XLA Ops:
  0.6 1.8 %broadcast_in_dim.16 = bf16[8,64,512]{2,1,0:T(8,128)(2,1)} broadcast(bf16[64,512]{1,0:T(8,128)(2,1)} %param.20), dimensions={1,2} | broadcast | bytes 589824 | tf_op jit(solution)/shard_map/broadcast_in_dim | solution.py:16
  2.4 4.6 %all-to-all-start = ((bf16[8,64,512]{2,1,0:T(8,128)(2,1)}), bf16[8,64,512]{2,1,0:T(8,128)(2,1)S(1)}, u32[]{:S(2)}, u32[]{:S(2)}) async-start(bf16[8,64,512]{2,1,0:T(8,128)(2,1)} %broadcast_in_dim.16), calls=%async_computation | async-start | bytes 1048576 | tf_op jit(solution)/shard_map/all_to_all | solution.py:15
  7.0 0.7 exp.13
  7.6 0.8 add_divide_fusion
  8.5 1.1 fusion.64
  9.6 7.7 %all-to-all-done = bf16[8,64,512]{2,1,0:T(8,128)(2,1)S(1)} async-done(((bf16[8,64,512]{2,1,0:T(8,128)(2,1)}), bf16[8,64,512]{2,1,0:T(8,128)(2,1)S(1)}, u32[]{:S(2)}, u32[]{:S(2)}) %all-to-all-start) | async-done | bytes 524320 | tf_op jit(solution)/shard_map/all_to_all | solution.py:15
  17.3 0.2 fusion.25
  17.8 0.4 convolution_convert_fusion.2
  18.4 0.2 copy-done.5
  18.5 0.2 fusion.15
  18.8 0.2 fusion.16
  19.1 0.2 fusion.65
  19.2 0.3 copy-done.1
  19.5 0.2 fusion.19
  19.8 0.7 broadcast_in_dim.17
  20.5 3.4 %all-to-all-start.1 = ((bf16[8,64,128]{2,1,0:T(8,128)(2,1)}), bf16[8,64,128]{2,1,0:T(8,128)(2,1)S(1)}, u32[]{:S(2)}, u32[]{:S(2)}) async-start(bf16[8,64,128]{2,1,0:T(8,128)(2,1)} %broadcast_in_dim.17), calls=%async_computation.1 | async-start | bytes 262144 | tf_op jit(solution)/shard_map/all_to_all | solution.py:15
  24.0 0.1 eq.28
  24.1 5.8 %all-to-all-done.1 = bf16[8,64,128]{2,1,0:T(8,128)(2,1)S(1)} async-done(((bf16[8,64,128]{2,1,0:T(8,128)(2,1)}), bf16[8,64,128]{2,1,0:T(8,128)(2,1)S(1)}, u32[]{:S(2)}, u32[]{:S(2)}) %all-to-all-start.1) | async-done | bytes 131104 | tf_op jit(solution)/shard_map/all_to_all | solution.py:15
  29.9 0.5 convolution_convert_fusion
  30.4 0.8 copy.145
  31.2 3.5 %all-to-all-start.2 = ((bf16[8,64,512]{2,1,0:T(8,128)(2,1)}), bf16[8,64,512]{2,1,0:T(8,128)(2,1)S(1)}, u32[]{:S(2)}, u32[]{:S(2)}) async-start(bf16[8,64,512]{2,1,0:T(8,128)(2,1)} %bitcast.94), calls=%async_computation.2 | async-start | bytes 1048576 | tf_op jit(solution)/shard_map/all_to_all | solution.py:38
  34.8 0.2 reduce_window_sum.11
  35.0 0.2 select_reduce_fusion.1
  35.2 0.1 reduce_sum.80
  35.4 9.6 %all-to-all-done.2 = bf16[8,64,512]{2,1,0:T(8,128)(2,1)S(1)} async-done(((bf16[8,64,512]{2,1,0:T(8,128)(2,1)}), bf16[8,64,512]{2,1,0:T(8,128)(2,1)S(1)}, u32[]{:S(2)}, u32[]{:S(2)}) %all-to-all-start.2) | async-done | bytes 524320 | tf_op jit(solution)/shard_map/all_to_all | solution.py:38
  45.2 0.6 broadcast_in_dim.20
  45.8 3.3 %all-to-all-start.3 = ((f32[8,1,64]{2,1,0:T(1,128)}), f32[8,1,64]{2,1,0:T(1,128)S(1)}, u32[]{:S(2)}, u32[]{:S(2)}) async-start(f32[8,1,64]{2,1,0:T(1,128)} %broadcast_in_dim.20), calls=%async_computation.3 | async-start | bytes 8192 | tf_op jit(solution)/shard_map/all_to_all | solution.py:15
  49.2 0.8 dynamic_slice.3
  50.0 4.2 %all-to-all-done.3 = f32[8,1,64]{2,1,0:T(1,128)S(1)} async-done(((f32[8,1,64]{2,1,0:T(1,128)}), f32[8,1,64]{2,1,0:T(1,128)S(1)}, u32[]{:S(2)}, u32[]{:S(2)}) %all-to-all-start.3) | async-done | bytes 2080 | tf_op jit(solution)/shard_map/all_to_all | solution.py:15
  54.2 0.3 convolution_convert_fusion.1
  54.5 16.4 %all_to_all.41 = bf16[16,16,512]{2,1,0:T(8,128)(2,1)S(1)} all-to-all(bf16[16,16,512]{2,1,0:T(8,128)(2,1)S(1)} %bitcast.105), channel_id=1, replica_groups=mesh['ep'=16,'tp'=8] {'ep'}, dimensions={0} | all-to-all | bytes 524288 | tf_op jit(solution)/shard_map/all_to_all | solution.py:136
  70.9 0.3 broadcast_in_dim.21
  71.2 29.9 %all_to_all.42 = bf16[8,16,16,512]{3,2,1,0:T(8,128)(2,1)S(1)} all-to-all(bf16[8,16,16,512]{3,2,1,0:T(8,128)(2,1)S(1)} %broadcast_in_dim.21), channel_id=1, replica_groups=mesh['ep'=16,'tp'=8] {'tp'}, dimensions={0} | all-to-all | bytes 4194304 | tf_op jit(solution)/shard_map/all_to_all | solution.py:15
  101.1 1.4 copy.116
  102.5 0.9 copy.126
  103.5 1.7 %fusion.4 = f32[256,704]{0,1:T(8,128)S(1)} fusion(bf16[256,4096]{1,0:T(8,128)(2,1)S(1)} %bitcast.101, bf16[1,4096,704]{1,2,0:T(8,128)(2,1)S(1)} %bitcast.114), kind=kOutput, calls=%fused_computation.4 | convolution fusion | flops 1476395008 | bytes 8585216 | tf_op jit(solution)/shard_map/dot_general | solution.py:140
  105.2 0.2 slice-done.3
  105.4 1.7 %fusion.12 = bf16[256,704]{0,1:T(8,128)(2,1)S(1)} fusion(bf16[256,4096]{1,0:T(8,128)(2,1)S(1)} %bitcast.102, bf16[1,4096,704]{1,2,0:T(8,128)(2,1)S(1)} %bitcast.116, f32[256,704]{0,1:T(8,128)S(1)} %fusion.4), kind=kOutput, calls=%fused_computation.12 | convolution fusion | flops 1477476352 | bytes 8945664 | tf_op jit(solution)/shard_map/dot_general | solution.py:141
  107.1 0.2 copy.117
  107.3 4.4 %fusion.6 = bf16[16,16,4096]{2,1,0:T(8,128)(2,1)S(1)} fusion(bf16[16,16,704]{2,1,0:T(8,128)(2,1)S(1)} %bitcast.110, bf16[1,704,4096]{2,1,0:T(8,128)(2,1)} %param.39), kind=kOutput, calls=%fused_computation.6 | convolution fusion | flops 1477443584 | bytes 8224768 | tf_op jit(solution)/shard_map/dot_general | solution.py:143
  111.7 0.3 copy.144
  112.0 29.7 %all_to_all.43 = bf16[8,16,16,512]{3,2,1,0:T(8,128)(2,1)S(1)} all-to-all(bf16[8,16,16,512]{3,2,1,0:T(8,128)(2,1)S(1)} %bitcast.97), channel_id=1, replica_groups=mesh['ep'=16,'tp'=8] {'tp'}, dimensions={0} | all-to-all | bytes 4194304 | tf_op jit(solution)/shard_map/all_to_all | solution.py:38
  141.7 1.1 reduce_sum.85
  142.8 3.5 %all-to-all-start.7 = ((bf16[16,16,512]{2,1,0:T(8,128)(2,1)}), bf16[16,16,512]{2,1,0:T(8,128)(2,1)S(1)}, u32[]{:S(2)}, u32[]{:S(2)}) async-start(bf16[16,16,512]{2,1,0:T(8,128)(2,1)} %reduce_sum.85), calls=%async_computation.7 | async-start | bytes 524288 | tf_op jit(solution)/shard_map/all_to_all | solution.py:147
  146.3 1.0 pad_maximum_fusion
  147.3 1.1 copy.119
  148.4 6.5 %all-to-all-done.7 = bf16[16,16,512]{2,1,0:T(8,128)(2,1)S(1)} async-done(((bf16[16,16,512]{2,1,0:T(8,128)(2,1)}), bf16[16,16,512]{2,1,0:T(8,128)(2,1)S(1)}, u32[]{:S(2)}, u32[]{:S(2)}) %all-to-all-start.7) | async-done | bytes 262176 | tf_op jit(solution)/shard_map/all_to_all | solution.py:147
  155.0 0.8 fusion.17
  (48 shorter events, 1.2 us)
Async XLA Ops:
  0.6 29.3 %copy-start = (bf16[128,4096]{1,0:T(8,128)(2,1)S(1)}, bf16[128,4096]{1,0:T(8,128)(2,1)}, u32[]{:S(2)}) copy-start(bf16[128,4096]{1,0:T(8,128)(2,1)} %param.36) | copy-start | bytes 3145732
  2.4 14.9 %all-to-all-start = ((bf16[8,64,512]{2,1,0:T(8,128)(2,1)}), bf16[8,64,512]{2,1,0:T(8,128)(2,1)S(1)}, u32[]{:S(2)}, u32[]{:S(2)}) async-start(bf16[8,64,512]{2,1,0:T(8,128)(2,1)} %broadcast_in_dim.16), calls=%async_computation | async-start | bytes 1048576 | tf_op jit(solution)/shard_map/all_to_all | solution.py:15
  9.6 8.2 %copy-start.2 = (bf16[4096,128]{1,0:T(8,128)(2,1)S(1)}, bf16[4096,128]{1,0:T(8,128)(2,1)}, u32[]{:S(2)}) copy-start(bf16[4096,128]{1,0:T(8,128)(2,1)} %param.26) | copy-start | bytes 3145732
  9.6 8.2 %copy-start.9 = (f32[4096]{0:T(1024)S(1)}, f32[4096]{0:T(1024)}, u32[]{:S(2)}) copy-start(f32[4096]{0:T(1024)} %param.24) | copy-start | bytes 49156
  17.7 0.8 copy-start.5
  17.7 0.9 copy-start.6
  17.8 1.3 copy-start.8
  17.8 1.7 %copy-start.7 = (f32[8,16,64]{2,1,0:T(8,128)S(1)}, f32[8,16,64]{2,1,0:T(8,128)}, u32[]{:S(2)}) copy-start(f32[8,16,64]{2,1,0:T(8,128)} %param.33) | copy-start | bytes 98308
  17.8 1.7 %copy-start.10 = (f32[8,16]{1,0:T(8,128)S(1)}, f32[8,16]{1,0:T(8,128)}, u32[]{:S(2)}) copy-start(f32[8,16]{1,0:T(8,128)} %param.34) | copy-start | bytes 1540
  18.2 5.6 %copy-start.11 = (s32[64,2]{0,1:T(2,128)S(1)}, s32[64,2]{0,1:T(2,128)}, u32[]{:S(2)}) copy-start(s32[64,2]{0,1:T(2,128)} %param.21) | copy-start | bytes 1540
  18.2 11.7 %copy-start.3 = (bf16[1024,128]{1,0:T(8,128)(2,1)S(1)}, bf16[1024,128]{1,0:T(8,128)(2,1)}, u32[]{:S(2)}) copy-start(bf16[1024,128]{1,0:T(8,128)(2,1)} %param.35) | copy-start | bytes 786436
  18.8 0.7 copy-start.1
  20.5 9.4 %all-to-all-start.1 = ((bf16[8,64,128]{2,1,0:T(8,128)(2,1)}), bf16[8,64,128]{2,1,0:T(8,128)(2,1)S(1)}, u32[]{:S(2)}, u32[]{:S(2)}) async-start(bf16[8,64,128]{2,1,0:T(8,128)(2,1)} %broadcast_in_dim.17), calls=%async_computation.1 | async-start | bytes 262144 | tf_op jit(solution)/shard_map/all_to_all | solution.py:15
  24.1 20.9 %copy-start.4 = (bf16[64,512]{1,0:T(8,128)(2,1)S(1)}, bf16[64,512]{1,0:T(8,128)(2,1)}, u32[]{:S(2)}) copy-start(bf16[64,512]{1,0:T(8,128)(2,1)} %param.20) | copy-start | bytes 196612
  30.4 18.7 %copy-start.12 = (f32[64,2]{0,1:T(2,128)S(1)}, f32[64,2]{0,1:T(2,128)}, u32[]{:S(2)}) copy-start(f32[64,2]{0,1:T(2,128)} %param.22) | copy-start | bytes 1540
  31.2 13.7 %all-to-all-start.2 = ((bf16[8,64,512]{2,1,0:T(8,128)(2,1)}), bf16[8,64,512]{2,1,0:T(8,128)(2,1)S(1)}, u32[]{:S(2)}, u32[]{:S(2)}) async-start(bf16[8,64,512]{2,1,0:T(8,128)(2,1)} %bitcast.94), calls=%async_computation.2 | async-start | bytes 1048576 | tf_op jit(solution)/shard_map/all_to_all | solution.py:38
  45.8 8.5 %all-to-all-start.3 = ((f32[8,1,64]{2,1,0:T(1,128)}), f32[8,1,64]{2,1,0:T(1,128)S(1)}, u32[]{:S(2)}, u32[]{:S(2)}) async-start(f32[8,1,64]{2,1,0:T(1,128)} %broadcast_in_dim.20), calls=%async_computation.3 | async-start | bytes 8192 | tf_op jit(solution)/shard_map/all_to_all | solution.py:15
  71.2 32.3 %slice-start = ((s8[5767168]{0:T(1024)(128)(4,1)}), s8[4194304]{0:T(1024)(128)(4,1)S(1)}, s32[]{:S(2)}) async-start(s8[5767168]{0:T(1024)(128)(4,1)} %bitcast.113), calls=%async_computation.8 | async-start | bytes 8388608
  101.1 2.3 %slice-start.1 = ((s8[5767168]{0:T(1024)(128)(4,1)}), s8[1572864]{0:T(1024)(128)(4,1)S(1)}, s32[]{:S(2)}) async-start(s8[5767168]{0:T(1024)(128)(4,1)} %bitcast.113), calls=%async_computation.9 | async-start | bytes 3145728
  102.5 2.7 %slice-start.2 = ((s8[5767168]{0:T(1024)(128)(4,1)}), s8[4194304]{0:T(1024)(128)(4,1)S(1)}, s32[]{:S(2)}) async-start(s8[5767168]{0:T(1024)(128)(4,1)} %bitcast.115), calls=%async_computation.10 | async-start | bytes 8388608
  103.4 2.0 %slice-start.3 = ((s8[5767168]{0:T(1024)(128)(4,1)}), s8[1572864]{0:T(1024)(128)(4,1)S(1)}, s32[]{:S(2)}) async-start(s8[5767168]{0:T(1024)(128)(4,1)} %bitcast.115), calls=%async_computation.11 | async-start | bytes 3145728
  142.8 12.2 %all-to-all-start.7 = ((bf16[16,16,512]{2,1,0:T(8,128)(2,1)}), bf16[16,16,512]{2,1,0:T(8,128)(2,1)S(1)}, u32[]{:S(2)}, u32[]{:S(2)}) async-start(bf16[16,16,512]{2,1,0:T(8,128)(2,1)} %reduce_sum.85), calls=%async_computation.7 | async-start | bytes 524288 | tf_op jit(solution)/shard_map/all_to_all | solution.py:147
where the time goes:
time: 157 us; the launch traced here: 156 us
  blocking collectives  75.9 us (48%)
  waiting for transfers between devices  33.9 us (22%)
  starting transfers between devices  18.3 us (12%)
  local copies, waits for them, and re-layouts  12 us (8%)
  matrix products  10.5 us (7%)
  other arithmetic  4.06 us (3%)
    all_to_all x1, blocking collectives, copy_for_each(): lax.all_to_all(jnp.broadcast_to(array[None], (size, *array.shape)), axis,...  29.9 us
    all_to_all x1, blocking collectives, sent_and_summed(): lax.all_to_all(blocks, axis, split_axis=0, concat_axis=0, tiled=True)  29.7 us
    all_to_all x3, waiting for transfers between devices, copy_for_each(): lax.all_to_all(jnp.broadcast_to(array[None], (size, *array.shape)), axis,...  17.7 us
    all_to_all x1, blocking collectives, per_device(): lax.all_to_all(outbound, 'ep', split_axis=0, concat_axis=0, tiled=True)  16.4 us
    all_to_all x3, starting transfers between devices, copy_for_each(): lax.all_to_all(jnp.broadcast_to(array[None], (size, *array.shape)), axis,...  11.3 us
    all_to_all x1, waiting for transfers between devices, sent_and_summed(): lax.all_to_all(blocks, axis, split_axis=0, concat_axis=0, tiled=True)  9.58 us
    all_to_all x1, waiting for transfers between devices, per_device(): lax.all_to_all(expert_out, 'ep', split_axis=0, concat_axis=0, tiled=True)  6.55 us
    dot_general x1, matrix products, per_device(): partial_sum = jnp.dot(hidden, w_down[0], preferred_element_type=jnp.float32)  4.43 us
  transfers between devices with their start and end apart: 5, of which 5 were waited for; matrix products, arithmetic and copies ran while one was open for 4% of the time, Pallas kernels for 0%

commit v1 on v0

v1 whole, which is shorter than its diff:
```python
import functools

import jax
import jax.numpy as jnp
from jax import lax
from jax.experimental import pallas as pl
from jax.experimental.pallas import tpu as pltpu
from jax.sharding import PartitionSpec as P

MESH = pl.DeviceIdType.MESH
BF = jnp.bfloat16
F32 = jnp.float32
EPS = 1e-06
NT = (((1,), (1,)), ((), ()))

NEP = 16
NTP = 8
ROWS = 64
WIDTH = 512
SLOT = 16
SLOTS = NEP * SLOT
FFW = 704
STATE = 64
GRP = 8
GCH = 16


def dot(a, b):
    return jnp.dot(a, b, preferred_element_type=F32)


def dot_nt(a, b):
    return lax.dot_general(a, b, NT, preferred_element_type=F32)


def iota(shape, dim):
    return lax.broadcasted_iota(jnp.int32, shape, dim)


def kernel(
    residual, routes, weights, state, mix_gain, ffn_gain, w_in, decay_rate, rotation,
    log_step, in_re, in_im, read_re, read_im, skip, w_glu, w_out, w_gate, w_up, w_down,
    out, state_out,
    v_routes, v_weights, v_state, v_mix, v_ffn, v_win, v_rate, v_rot, v_step, v_inre,
    v_inim, v_rre, v_rim, v_skip, v_glu, v_out, v_gate, v_up, v_down,
    g1, bd_hi, bd_lo, rbd, fresh, new_state, act_all, act32, mixed,
    b_ds, b_dr, b_q, b_own, b_rel, b_dir, b_mrg, b_ms,
    after, d_map, wt, outb, g2, acc_g, acc_u, sq, hidden,
    e_ds, e_dr, e_q, e_own, e_rel, e_dir, e_mrg, e_ms, eout, back, v_layer,
    load_sem, g1_s, g1_r, a_s, a_r, b_s, b_r, x_s, x_r, g2_s, g2_r, e_s, e_r, ret_s, ret_r, st_sem,
):
    ep = lax.axis_index("ep")
    tp = lax.axis_index("tp")
    y, c = lax.div(tp, 2), lax.rem(tp, 2)
    z, x = lax.div(ep, 4), lax.rem(ep, 4)
    yp, ym, yo = lax.rem(y + 1, 4), lax.rem(y + 3, 4), lax.rem(y + 2, 4)
    oc = 1 - c
    partner = y * 2 + oc
    up, down = yp * 2 + c, ym * 2 + c
    sent = []

    def send(src, dst, ss, rs, device):
        copy = pltpu.make_async_remote_copy(
            src_ref=src, dst_ref=dst, send_sem=ss, recv_sem=rs, device_id=device, device_id_type=MESH
        )
        copy.start()
        sent.append(copy)

    def arrive(dst, ss, rs):
        pltpu.make_async_remote_copy(
            src_ref=dst, dst_ref=dst, send_sem=ss, recv_sem=rs, device_id=(ep, partner), device_id_type=MESH
        ).wait_recv()

    pairs = [
        (residual, g1.at[tp]), (w_in, v_win), (mix_gain, v_mix),
        (decay_rate, v_rate), (rotation, v_rot), (log_step, v_step), (in_re, v_inre), (in_im, v_inim),
        (read_re, v_rre), (read_im, v_rim), (skip, v_skip), (routes, v_routes), (weights, v_weights),
        (state, v_state), (w_glu, v_glu), (w_out, v_out), (ffn_gain, v_ffn),
        (w_gate, v_gate), (w_up, v_up), (w_down, v_down),
    ]
    loads = [pltpu.make_async_copy(src, dst, load_sem.at[i]) for i, (src, dst) in enumerate(pairs)]
    for load in loads:
        load.start()

    barrier = pltpu.get_barrier_semaphore()
    for d in range(1, NTP):
        pl.semaphore_signal(barrier, inc=1, device_id=(ep, lax.rem(tp + d, NTP)), device_id_type=MESH)
    for d in range(1, NEP):
        pl.semaphore_signal(barrier, inc=1, device_id=(lax.rem(ep + d, NEP), tp), device_id_type=MESH)

    for i in range(3, 14):
        loads[i].wait()

    eye8 = iota((GRP, GRP), 0) == iota((GRP, GRP), 1)
    step = jnp.exp(jnp.sum(jnp.where(eye8, jnp.broadcast_to(v_step[...], (GRP, GRP)), 0.0), axis=1, keepdims=True))
    rate, rot = v_rate[...], v_rot[...]
    real = -rate
    magnitude = jnp.exp(real * step)
    angle = rot * step
    decay_re = magnitude * jnp.cos(angle)
    decay_im = magnitude * jnp.sin(angle)
    denominator = real * real + rot * rot
    lift_re = ((decay_re - 1.0) * real + decay_im * rot) / denominator
    lift_im = (decay_im * real - (decay_re - 1.0) * rot) / denominator
    bd_hi[...] = jnp.zeros_like(bd_hi)
    bd_lo[...] = jnp.zeros_like(bd_lo)
    rbd[...] = jnp.zeros_like(rbd)
    fresh[...] = jnp.zeros_like(fresh)
    for g in range(GRP):
        rows = slice(g * GCH, (g + 1) * GCH)
        l_re, l_im = lift_re[g:g + 1, :], lift_im[g:g + 1, :]
        b_re, b_im = v_inre[rows, :], v_inim[rows, :]
        for n, value in enumerate((l_re * b_re - l_im * b_im, l_re * b_im + l_im * b_re)):
            lanes = slice((2 * g + n) * 128, (2 * g + n) * 128 + STATE)
            hi = value.astype(BF)
            bd_hi[rows, lanes] = hi
            bd_lo[rows, lanes] = (value - hi.astype(F32)).astype(BF)
        rbd[rows, (2 * g) * 128:(2 * g) * 128 + STATE] = v_rre[rows, :].astype(BF)
        rbd[rows, (2 * g + 1) * 128:(2 * g + 1) * 128 + STATE] = (-v_rim[rows, :]).astype(BF)
    tiler = (iota((GCH, 128), 0) == lax.rem(iota((GCH, 128), 1), GCH)).astype(BF)
    skip_hi = v_skip[...].astype(BF)
    skip_rest = v_skip[...] - skip_hi.astype(F32)
    skip_mid = skip_rest.astype(BF)
    skip_lo = (skip_rest - skip_mid.astype(F32)).astype(BF)
    skip_rep = dot(skip_hi, tiler) + dot(skip_mid, tiler) + dot(skip_lo, tiler)
    skip_row = jnp.sum(
        jnp.where(lax.div(iota((GRP, 128), 1), GCH) == iota((GRP, 128), 0), skip_rep, 0.0), axis=0, keepdims=True
    )
    r0, r1 = v_routes[0:1, :], v_routes[1:2, :]
    oh0 = (r0 == iota((NEP, ROWS), 0)).astype(F32)
    oh1 = (r1 == iota((NEP, ROWS), 0)).astype(F32)
    upper_tri = (iota((ROWS, ROWS), 0) < iota((ROWS, ROWS), 1)).astype(BF)
    before = dot((oh0 + oh1).astype(BF), upper_tri)
    dest0 = r0.astype(F32) * SLOT + jnp.sum(before * oh0, axis=0, keepdims=True)
    dest1 = r1.astype(F32) * SLOT + jnp.sum(before * oh1, axis=0, keepdims=True)
    place = iota((SLOTS, ROWS), 0).astype(F32)
    m0, m1 = (dest0 == place).astype(F32), (dest1 == place).astype(F32)
    d_map[...] = (m0 + m1).astype(BF)
    w_all = jnp.transpose(v_weights[0:1, :] * m0 + v_weights[1:2, :] * m1)
    w_hi = w_all.astype(BF)
    wt[0] = w_hi
    wt[1] = (w_all - w_hi.astype(F32)).astype(BF)

    def gather_send(buf, half, ss, rs, rows):
        send(buf(tp, *rows), buf(tp, *rows), ss(0), rs(0), (ep, up))
        send(buf(tp, *rows), buf(tp, *rows), ss(1), rs(1), (ep, down))
        send(buf(tp, *rows), buf(tp, *rows), ss(4), rs(4), (ep, partner))

    def gather_relay(buf, half, ss, rs, rows):
        first, size = rows
        lo_half, hi_half = (first, half), (first + half, half)
        arrive(buf(down, *rows), ss(0), rs(0))
        send(buf(down, *lo_half), buf(down, *lo_half), ss(2), rs(2), (ep, up))
        send(buf(down, *rows), buf(down, *rows), ss(5), rs(5), (ep, partner))
        arrive(buf(up, *rows), ss(1), rs(1))
        send(buf(up, *hi_half), buf(up, *hi_half), ss(3), rs(3), (ep, down))
        send(buf(up, *rows), buf(up, *rows), ss(6), rs(6), (ep, partner))

    far, far_oc = yo * 2 + c, yo * 2 + oc
    up_oc, down_oc = yp * 2 + oc, ym * 2 + oc

    def gather_far(buf, half, ss, rs, rows):
        first, size = rows
        lo_half, hi_half = (first, half), (first + half, half)
        arrive(buf(far, *lo_half), ss(2), rs(2))
        send(buf(far, *lo_half), buf(far, *lo_half), ss(7), rs(7), (ep, partner))
        arrive(buf(far, *hi_half), ss(3), rs(3))
        send(buf(far, *hi_half), buf(far, *hi_half), ss(8), rs(8), (ep, partner))

    def at1(t, first, size):
        return g1.at[t, pl.ds(first, size), :]

    one = (at1, ROWS // 2, lambda k: g1_s.at[k], lambda k: g1_r.at[k], (0, ROWS))
    loads[0].wait()
    pl.semaphore_wait(barrier, NTP + NEP - 2)
    gather_send(*one)
    loads[1].wait()
    loads[2].wait()

    total = [None, None]

    def mix_block(t):
        rows = g1[t].astype(F32)
        squares = jnp.sum(rows * rows, axis=1, keepdims=True)
        gain = v_mix[:, pl.ds(pl.multiple_of(t * WIDTH, WIDTH), WIDTH)]
        product = dot((rows * gain).astype(BF), v_win[pl.ds(pl.multiple_of(t * WIDTH, WIDTH), WIDTH), :])
        total[0] = squares if total[0] is None else total[0] + squares
        total[1] = product if total[1] is None else total[1] + product

    mix_block(tp)
    gather_relay(*one)
    mix_block(down)
    mix_block(up)
    arrive(at1(partner, 0, ROWS), g1_s.at[4], g1_r.at[4])
    mix_block(partner)
    gather_far(*one)
    arrive(at1(down_oc, 0, ROWS), g1_s.at[5], g1_r.at[5])
    mix_block(down_oc)
    arrive(at1(up_oc, 0, ROWS), g1_s.at[6], g1_r.at[6])
    mix_block(up_oc)
    mix_block(far)
    arrive(at1(far_oc, 0, ROWS // 2), g1_s.at[7], g1_r.at[7])
    arrive(at1(far_oc, ROWS // 2, ROWS // 2), g1_s.at[8], g1_r.at[8])
    mix_block(far_oc)
    u_in = (total[1] * lax.rsqrt(total[0] / (NTP * WIDTH) + EPS)).astype(BF)

    drive = dot(u_in, bd_hi[...]) + dot(u_in, bd_lo[...])
    for g in range(GRP):
        old_re = v_state[pl.ds(g, ROWS, stride=2 * GRP), :]
        old_im = v_state[pl.ds(GRP + g, ROWS, stride=2 * GRP), :]
        k_re, k_im = decay_re[g:g + 1, :], decay_im[g:g + 1, :]
        new_re = k_re * old_re - k_im * old_im + drive[:, (2 * g) * 128:(2 * g) * 128 + STATE]
        new_im = k_re * old_im + k_im * old_re + drive[:, (2 * g + 1) * 128:(2 * g + 1) * 128 + STATE]
        new_state[pl.ds(g, ROWS, stride=2 * GRP), :] = new_re
        new_state[pl.ds(GRP + g, ROWS, stride=2 * GRP), :] = new_im
        fresh[:, (2 * g) * 128:(2 * g) * 128 + STATE] = new_re.astype(BF)
        fresh[:, (2 * g + 1) * 128:(2 * g + 1) * 128 + STATE] = new_im.astype(BF)
    act = jax.nn.gelu(dot_nt(fresh[...], rbd[...]) + skip_row * u_in.astype(F32))
    act32[...] = act
    act_all[tp] = act.astype(BF)
    for d in range(1, NTP):
        send(act_all.at[tp], act_all.at[tp], a_s.at[d], a_r.at[d], (ep, lax.rem(tp + d, NTP)))
    store_state = pltpu.make_async_copy(new_state, state_out, st_sem)
    store_state.start()
    loads[14].wait()
    loads[15].wait()
    for d in range(1, NTP):
        arrive(act_all.at[lax.rem(tp + NTP - d, NTP)], a_s.at[d], a_r.at[d])
    logit = dot(jnp.concatenate([act_all[t] for t in range(NTP)], axis=1), v_glu[...])
    mixed[...] = (act32[...] * jax.nn.sigmoid(logit)).astype(BF)

    order = (yo, yp, ym, y)

    def reduce_scatter(product, rows, sets, ds, dr, q, own, rel, dire, mrg, ms, ss, rs, done):
        half = rows // 2
        piece = half // sets
        base = 4

        def lo(i):
            return pl.ds(i * piece, piece)

        def hi(i):
            return pl.ds(half + i * piece, piece)

        def sem(kind, i):
            return base + kind * sets + i

        for j in range(4):
            ds[j] = product(order[j] * 2 + oc).astype(BF)
            send(ds.at[j], dr.at[j], ss.at[j], rs.at[j], (ep, partner))

        def on_chip(j):
            value = product(order[j] * 2 + c)
            arrive(dr.at[j], ss.at[j], rs.at[j])
            return value + dr[j].astype(F32)

        q[0] = on_chip(0).astype(BF)
        for i in range(sets):
            send(q.at[0, lo(i), :], rel.at[0, lo(i), :], ss.at[sem(0, i)], rs.at[sem(0, i)], (ep, up))
            send(q.at[0, hi(i), :], rel.at[1, lo(i), :], ss.at[sem(1, i)], rs.at[sem(1, i)], (ep, down))
        q[1] = on_chip(1).astype(BF)

        def direct_up(i):
            send(q.at[1, hi(i), :], dire.at[0, lo(i), :], ss.at[sem(2, i)], rs.at[sem(2, i)], (ep, up))

        def direct_down(i):
            send(q.at[2, lo(i), :], dire.at[1, lo(i), :], ss.at[sem(3, i)], rs.at[sem(3, i)], (ep, down))

        direct_up(0)
        q[2] = on_chip(2).astype(BF)
        direct_down(0)
        own[...] = on_chip(3)
        for i in range(sets):
            if i:
                direct_up(i)
                direct_down(i)
            arrive(rel.at[0, lo(i), :], ss.at[sem(0, i)], rs.at[sem(0, i)])
            ms[0, i * piece:(i + 1) * piece, :] = (
                q[1, i * piece:(i + 1) * piece, :].astype(F32) + rel[0, i * piece:(i + 1) * piece, :].astype(F32)
            ).astype(BF)
            send(ms.at[0, lo(i), :], mrg.at[0, lo(i), :], ss.at[sem(4, i)], rs.at[sem(4, i)], (ep, up))
            arrive(rel.at[1, lo(i), :], ss.at[sem(1, i)], rs.at[sem(1, i)])
            ms[1, i * piece:(i + 1) * piece, :] = (
                q[2, half + i * piece:half + (i + 1) * piece, :].astype(F32)
                + rel[1, i * piece:(i + 1) * piece, :].astype(F32)
            ).astype(BF)
            send(ms.at[1, lo(i), :], mrg.at[1, lo(i), :], ss.at[sem(5, i)], rs.at[sem(5, i)], (ep, down))
        for i in range(sets):
            part = slice(i * piece, (i + 1) * piece)
            arrive(dire.at[1, lo(i), :], ss.at[sem(3, i)], rs.at[sem(3, i)])
            arrive(mrg.at[0, lo(i), :], ss.at[sem(4, i)], rs.at[sem(4, i)])
            done(i * piece, piece, own[part, :] + dire[1, part, :].astype(F32) + mrg[0, part, :].astype(F32))
            top = slice(half + i * piece, half + (i + 1) * piece)
            arrive(dire.at[0, lo(i), :], ss.at[sem(2, i)], rs.at[sem(2, i)])
            arrive(mrg.at[1, lo(i), :], ss.at[sem(5, i)], rs.at[sem(5, i)])
            done(half + i * piece, piece, own[top, :] + dire[0, part, :].astype(F32) + mrg[1, part, :].astype(F32))

    def columns(t):
        return pl.ds(pl.multiple_of(t * WIDTH, WIDTH), WIDTH)

    def branch_done(first, size, value):
        source = g1[tp, first:first + size, :].astype(F32)
        after[first:first + size, :] = (source + value).astype(BF)

    reduce_scatter(
        lambda t: dot(mixed[...], v_out[:, columns(t)]), ROWS, 1,
        b_ds, b_dr, b_q, b_own, b_rel, b_dir, b_mrg, b_ms, b_s, b_r, branch_done,
    )

    outb[...] = dot(d_map[...], after[...]).astype(BF)

    def slot(e):
        return pl.ds(pl.multiple_of(e * SLOT, SLOT), SLOT)

    hops = [(dz, dx) for dz in (0, 1, 3, 2) for dx in (1, 3, 2, 0) if (dz, dx) != (0, 0)]
    for dz, dx in hops:
        k = dz * 4 + dx
        e = lax.rem(z + dz, 4) * 4 + lax.rem(x + dx, 4)
        send(outb.at[slot(e), :], g2.at[tp, slot(ep), :], x_s.at[k], x_r.at[k], (e, tp))
    g2[tp, slot(ep), :] = outb[slot(ep), :]
    loads[16].wait()
    loads[17].wait()
    loads[18].wait()

    def at2(t, first, size):
        return g2.at[t, pl.ds(first, size), :]

    def sems2(table, j):
        return lambda k: table.at[j, k]

    chunk = SLOTS // 4
    turns = (0, 1, 3, 2)
    plans = []
    for j, dz in enumerate(turns):
        first = pl.multiple_of(lax.rem(z + 4 - dz, 4) * chunk, chunk)
        plans.append((at2, chunk // 2, sems2(g2_s, j), sems2(g2_r, j), (first, chunk)))

    def start_chunk(j):
        dz = turns[j]
        for dx in (1, 3, 2, 0):
            if (dz, dx) == (0, 0):
                continue
            k = dz * 4 + dx
            s = lax.rem(z + 4 - dz, 4) * 4 + lax.rem(x + 4 - dx, 4)
            arrive(g2.at[tp, slot(s), :], x_s.at[k], x_r.at[k])
        gather_send(*plans[j])

    began = []

    def expert_block(t):
        gain = v_ffn[:, columns(t)]
        rows = g2[t].astype(F32)
        scaled = (rows * gain).astype(BF)
        squares = rows * rows
        squares = squares[:, 0:128] + squares[:, 128:256] + squares[:, 256:384] + squares[:, 384:512]
        gate, upper = dot_nt(scaled, v_gate[:, columns(t)]), dot_nt(scaled, v_up[:, columns(t)])
        if began:
            sq[...] += squares
            acc_g[...] += gate
            acc_u[...] += upper
        else:
            began.append(True)
            sq[...] = squares
            acc_g[...] = gate
            acc_u[...] = upper

    def from_partner(t, kinds):
        for j in range(4):
            at, half, ss, rs, (first, size) = plans[j]
            if len(kinds) == 1:
                arrive(at(t, first, size), ss(kinds[0]), rs(kinds[0]))
            else:
                arrive(at(t, first, half), ss(kinds[0]), rs(kinds[0]))
                arrive(at(t, first + half, half), ss(kinds[1]), rs(kinds[1]))

    start_chunk(0)
    start_chunk(1)
    gather_relay(*plans[0])
    start_chunk(2)
    gather_relay(*plans[1])
    gather_far(*plans[0])
    start_chunk(3)
    gather_relay(*plans[2])
    gather_far(*plans[1])
    expert_block(tp)
    gather_relay(*plans[3])
    from_partner(partner, (4,))
    expert_block(partner)
    gather_far(*plans[2])
    expert_block(down)
    expert_block(up)
    gather_far(*plans[3])
    from_partner(down_oc, (5,))
    expert_block(down_oc)
    from_partner(up_oc, (6,))
    expert_block(up_oc)
    expert_block(far)
    from_partner(far_oc, (7, 8))
    expert_block(far_oc)

    loads[19].wait()
    for r in range(0, SLOTS, 64):
        scale = lax.rsqrt(jnp.sum(sq[r:r + 64, :], axis=1, keepdims=True) / (NTP * WIDTH) + EPS)
        gate, upper = acc_g[r:r + 64, :] * scale, acc_u[r:r + 64, :] * scale
        hidden[r:r + 64, :] = (gate * jax.nn.sigmoid(gate) * upper).astype(BF)

    def expert_done(first, size, value):
        eout[first:first + size, :] = value.astype(BF)
        for s in range(first // SLOT, (first + size) // SLOT):
            rows = slice(s * SLOT, (s + 1) * SLOT)

            @pl.when(ep == s)
            def _():
                back[rows, :] = eout[rows, :]

            @pl.when(ep != s)
            def _():
                pltpu.make_async_remote_copy(
                    src_ref=eout.at[pl.ds(s * SLOT, SLOT), :], dst_ref=back.at[slot(ep), :],
                    send_sem=ret_s.at[s], recv_sem=ret_r.at[ep], device_id=(s, tp), device_id_type=MESH,
                ).start()

    reduce_scatter(
        lambda t: dot(hidden[...], v_down[:, columns(t)]), SLOTS, 2,
        e_ds, e_dr, e_q, e_own, e_rel, e_dir, e_mrg, e_ms, e_s, e_r, expert_done,
    )
    for d in range(1, NEP):
        e = lax.rem(ep + d, NEP)
        arrive(back.at[slot(e), :], ret_s.at[e], ret_r.at[e])
    combined = dot(wt[0], back[...]) + dot(wt[1], back[...])
    v_layer[...] = (after[...].astype(F32) + combined).astype(BF)
    finish = pltpu.make_async_copy(v_layer, out, load_sem.at[0])
    finish.start()
    for copy in sent:
        copy.wait_send()
    for d in range(1, NEP):
        e = lax.rem(ep + d, NEP)
        pltpu.make_async_remote_copy(
            src_ref=eout.at[slot(e), :], dst_ref=eout.at[slot(e), :], send_sem=ret_s.at[e], recv_sem=ret_r.at[e],
            device_id=(e, tp), device_id_type=MESH,
        ).wait_send()
    store_state.wait()
    finish.wait()


def per_device(
    residual, routes, route_weights, state_prev, mix_gain, ffn_gain, w_in, decay_rate, rotation,
    log_step, in_re, in_im, read_re, read_im, skip_gain, w_glu, w_out, w_gate, w_up, w_down,
):
    dma = pltpu.SemaphoreType.DMA
    vm = pltpu.VMEM
    operands = (
        residual, routes.T, route_weights.T, state_prev.reshape(ROWS * 2 * GRP, STATE), mix_gain.reshape(1, -1),
        ffn_gain.reshape(1, -1), w_in, decay_rate, rotation, log_step.reshape(1, GRP),
        in_re.transpose(0, 2, 1).reshape(GRP * GCH, STATE), in_im.transpose(0, 2, 1).reshape(GRP * GCH, STATE), read_re.reshape(GRP * GCH, STATE),
        read_im.reshape(GRP * GCH, STATE), skip_gain, w_glu, w_out, w_gate[0].T, w_up[0].T, w_down[0],
    )

    def exchange(rows):
        half = rows // 2
        return [
            vm((4, rows, WIDTH), BF), vm((4, rows, WIDTH), BF), vm((3, rows, WIDTH), BF), vm((rows, WIDTH), F32),
            vm((2, half, WIDTH), BF), vm((2, half, WIDTH), BF), vm((2, half, WIDTH), BF), vm((2, half, WIDTH), BF),
        ]

    scratch = [vm(operands[i].shape, operands[i].dtype) for i in range(1, 20)]
    scratch += [
        vm((NTP, ROWS, WIDTH), BF), vm((128, 2048), BF), vm((128, 2048), BF),
        vm((128, 2048), BF), vm((ROWS, 2048), BF), vm((ROWS * 2 * GRP, STATE), F32), vm((NTP, ROWS, 128), BF),
        vm((ROWS, 128), F32), vm((ROWS, 128), BF),
    ]
    scratch += exchange(ROWS)
    scratch += [
        vm((ROWS, WIDTH), BF), vm((SLOTS, ROWS), BF), vm((2, ROWS, SLOTS), BF), vm((SLOTS, WIDTH), BF),
        vm((NTP, SLOTS, WIDTH), BF), vm((SLOTS, FFW), F32), vm((SLOTS, FFW), F32), vm((SLOTS, 128), F32),
        vm((SLOTS, FFW), BF),
    ]
    scratch += exchange(SLOTS)
    scratch += [vm((SLOTS, WIDTH), BF), vm((SLOTS, WIDTH), BF), vm((ROWS, WIDTH), BF)]
    scratch += [
        dma((20,)), dma((9,)), dma((9,)), dma((8,)), dma((8,)), dma((10,)), dma((10,)), dma((16,)), dma((16,)),
        dma((4, 9)), dma((4, 9)), dma((16,)), dma((16,)), dma((16,)), dma((16,)), dma,
    ]
    anywhere = pl.BlockSpec(memory_space=pl.ANY)
    layer_out, state_next = pl.pallas_call(
        kernel,
        out_shape=(
            jax.ShapeDtypeStruct((ROWS, WIDTH), BF),
            jax.ShapeDtypeStruct((ROWS * 2 * GRP, STATE), F32),
        ),
        in_specs=[anywhere] * 20,
        out_specs=(anywhere, anywhere),
        scratch_shapes=scratch,
        compiler_params=pltpu.CompilerParams(
            collective_id=0, has_side_effects=True, vmem_limit_bytes=60 * 1024 * 1024
        ),
        name="layer",
    )(*operands)
    return layer_out, state_next.reshape(ROWS, 2, GRP, STATE)


def solution(mesh):
    return jax.shard_map(
        per_device,
        mesh=mesh,
        in_specs=(
            P("ep", "tp"), P("ep", None), P("ep", None), P("ep", None, "tp", None), P(), P(), P(None, "tp"),
            P("tp", None), P("tp", None), P("tp"), P("tp", None, None), P("tp", None, None), P("tp", None, None),
            P("tp", None, None), P("tp", None), P(None, "tp"), P("tp", None), P("ep", None, "tp"),
            P("ep", None, "tp"), P("ep", "tp", None),
        ),
        out_specs=(P("ep", "tp"), P("ep", None, "tp", None)),
        check_vma=False,
    )
```

time: 157 us -> 74.4 us (0.47)
  blocking collectives: 75.9 us -> 0 us
  Pallas kernels: 0 us -> 69.4 us
  waiting for transfers between devices: 33.9 us -> 0 us
  starting transfers between devices: 18.3 us -> 0 us
  matrix products: 10.5 us -> 0 us
  local copies, waits for them, and re-layouts: 12 us -> 3.34 us
  other arithmetic: 4.06 us -> 0 us
    all_to_all x3 -> x0, blocking collectives: 75.9 us -> none  [the longest x1 29.9 us: copy_for_each(): lax.all_to_all(jnp.broadcast_to(array[None], (size, *array.shape)), axis,...]
    pallas_call x0 -> x1, Pallas kernels: none -> 69.4 us  [per_device(): pl.pallas_call(kernel, out_shape=(jax.ShapeDtypeStruct((ROWS, WIDTH), BF)...]
    all_to_all x5 -> x0, waiting for transfers between devices: 33.9 us -> none  [the longest x3 17.7 us: copy_for_each(): lax.all_to_all(jnp.broadcast_to(array[None], (size, *array.shape)), axis,...]
    all_to_all x5 -> x0, starting transfers between devices: 18.3 us -> none  [the longest x3 11.3 us: copy_for_each(): lax.all_to_all(jnp.broadcast_to(array[None], (size, *array.shape)), axis,...]
    dot_general x11 -> x0, matrix products: 10.5 us -> none  [the longest x1 4.43 us: per_device(): partial_sum = jnp.dot(hidden, w_down[0], preferred_element_type=jnp.float32)]
    broadcast_in_dim x4 -> x0, local copies, waits for them, and re-layouts: 3.29 us -> none  [copy_for_each(): jnp.broadcast_to(array[None], (size, *array.shape))]
    reduce_sum x7 -> x0, other arithmetic: 1.78 us -> none  [the longest x2 1.16 us: sent_and_summed(): return arrived.astype(jnp.float32).sum(axis=0)]
    unnamed x37 -> x2, local copies, waits for them, and re-layouts: 2.9 us -> 3.34 us
  transfers between devices with their start and end apart: 5 -> 0, of which waited for: 5 -> 0; matrix products, arithmetic and copies ran while one was open for 4% -> 0% of each run, Pallas kernels for 0% -> 0%
where the time goes in v1:
time: 74.4 us; the launch traced here: 73.4 us
  Pallas kernels  69.4 us (93%)
  local copies, waits for them, and re-layouts  3.34 us (4%)
    pallas_call x1, Pallas kernels, per_device(): pl.pallas_call(kernel, out_shape=(jax.ShapeDtypeStruct((ROWS, WIDTH), BF)...  69.4 us
    unnamed x2, local copies, waits for them, and re-layouts  3.34 us

profile of v1, /device:TPU:0, one launch (start us, length us, event | category | flops | bytes accessed | tf_op | source)
XLA Modules:
  0.0 73.4 jit_solution(16419123165197986381)
XLA Ops:
  0.6 69.4 %layer.1 = (bf16[64,512]{1,0:T(8,128)(2,1)}, f32[1024,64]{1,0:T(8,128)}) custom-call(bf16[64,512]{1,0:T(8,128)(2,1)} %residual.1, s32[2,64]{1,0:T(2,128)} %bitcast.33, f32[2,64]{1,0:T(2,128)} %bitcast.34, f32[1024,64]{1,0:T(8,128)} %bitcast.25, f32[1,4096]{1,0:T(1,128)} %bitcast.31, f32[1,4096]{1,0:T(1,128)} %bitcast.32, bf16[4096,128]{1,0:T(8,128)(2,1)} %w_in.1, ...), custom_call_target="tpu_custom_call" | custom-call | tf_op jit(solution)/shard_map/layer/pallas_call | solution.py:485
  70.0 1.5 %copy.24 = bf16[64,512]{1,0:T(8,128)(2,1)} copy(bf16[64,512]{1,0:T(8,128)(2,1)} %get-tuple-element.8) | data formatting | bytes 131072
  71.5 1.9 %copy.25 = f32[64,2,8,64]{3,2,1,0:T(8,128)} copy(f32[64,2,8,64]{3,2,1,0:T(8,128)} %bitcast.26) | data formatting | bytes 524288

commit v2 on v1

--- a/solution.py
+++ b/solution.py
@@ -43,11 +43,11 @@
     out, state_out,
     v_routes, v_weights, v_state, v_mix, v_ffn, v_win, v_rate, v_rot, v_step, v_inre,
     v_inim, v_rre, v_rim, v_skip, v_glu, v_out, v_gate, v_up, v_down,
-    g1, bd_hi, bd_lo, rbd, fresh, new_state, act_all, act32, mixed,
+    g1, bd_hi, bd_lo, rbd, fresh, act_all, act32, mixed,
     b_ds, b_dr, b_q, b_own, b_rel, b_dir, b_mrg, b_ms,
     after, d_map, wt, outb, g2, acc_g, acc_u, sq, hidden,
-    e_ds, e_dr, e_q, e_own, e_rel, e_dir, e_mrg, e_ms, eout, back, v_layer,
-    load_sem, g1_s, g1_r, a_s, a_r, b_s, b_r, x_s, x_r, g2_s, g2_r, e_s, e_r, ret_s, ret_r, st_sem,
+    e_ds, e_dr, e_q, e_own, e_rel, e_dir, e_mrg, e_ms, eout, back,
+    load_sem, g1_s, g1_r, a_s, a_r, b_s, b_r, x_s, x_r, g2_s, g2_r, e_s, e_r, ret_s, ret_r,
 ):
     ep = lax.axis_index("ep")
     tp = lax.axis_index("tp")
@@ -79,8 +79,7 @@
         (w_gate, v_gate), (w_up, v_up), (w_down, v_down),
     ]
     loads = [pltpu.make_async_copy(src, dst, load_sem.at[i]) for i, (src, dst) in enumerate(pairs)]
-    for load in loads:
-        load.start()
+    loads[0].start()
 
     barrier = pltpu.get_barrier_semaphore()
     for d in range(1, NTP):
@@ -88,6 +87,42 @@
     for d in range(1, NEP):
         pl.semaphore_signal(barrier, inc=1, device_id=(lax.rem(ep + d, NEP), tp), device_id_type=MESH)
 
+    for load in loads[1:]:
+        load.start()
+
+    def gather_send(buf, half, ss, rs, rows):
+        send(buf(tp, *rows), buf(tp, *rows), ss(0), rs(0), (ep, up))
+        send(buf(tp, *rows), buf(tp, *rows), ss(1), rs(1), (ep, down))
+        send(buf(tp, *rows), buf(tp, *rows), ss(4), rs(4), (ep, partner))
+
+    def gather_relay(buf, half, ss, rs, rows):
+        first, size = rows
+        lo_half, hi_half = (first, half), (first + half, half)
+        arrive(buf(down, *rows), ss(0), rs(0))
+        send(buf(down, *lo_half), buf(down, *lo_half), ss(2), rs(2), (ep, up))
+        send(buf(down, *rows), buf(down, *rows), ss(5), rs(5), (ep, partner))
+        arrive(buf(up, *rows), ss(1), rs(1))
+        send(buf(up, *hi_half), buf(up, *hi_half), ss(3), rs(3), (ep, down))
+        send(buf(up, *rows), buf(up, *rows), ss(6), rs(6), (ep, partner))
+
+    far, far_oc = yo * 2 + c, yo * 2 + oc
+    up_oc, down_oc = yp * 2 + oc, ym * 2 + oc
+
+    def gather_far(buf, half, ss, rs, rows):
+        first, size = rows
+        lo_half, hi_half = (first, half), (first + half, half)
+        arrive(buf(far, *lo_half), ss(2), rs(2))
+        send(buf(far, *lo_half), buf(far, *lo_half), ss(7), rs(7), (ep, partner))
+        arrive(buf(far, *hi_half), ss(3), rs(3))
+        send(buf(far, *hi_half), buf(far, *hi_half), ss(8), rs(8), (ep, partner))
+
+    def at1(t, first, size):
+        return g1.at[t, pl.ds(first, size), :]
+
+    one = (at1, ROWS // 2, lambda k: g1_s.at[k], lambda k: g1_r.at[k], (0, ROWS))
+    loads[0].wait()
+    pl.semaphore_wait(barrier, NTP + NEP - 2)
+    gather_send(*one)
     for i in range(3, 14):
         loads[i].wait()
 
@@ -141,39 +176,6 @@
     wt[0] = w_hi
     wt[1] = (w_all - w_hi.astype(F32)).astype(BF)
 
-    def gather_send(buf, half, ss, rs, rows):
-        send(buf(tp, *rows), buf(tp, *rows), ss(0), rs(0), (ep, up))
-        send(buf(tp, *rows), buf(tp, *rows), ss(1), rs(1), (ep, down))
-        send(buf(tp, *rows), buf(tp, *rows), ss(4), rs(4), (ep, partner))
-
-    def gather_relay(buf, half, ss, rs, rows):
-        first, size = rows
-        lo_half, hi_half = (first, half), (first + half, half)
-        arrive(buf(down, *rows), ss(0), rs(0))
-        send(buf(down, *lo_half), buf(down, *lo_half), ss(2), rs(2), (ep, up))
-        send(buf(down, *rows), buf(down, *rows), ss(5), rs(5), (ep, partner))
-        arrive(buf(up, *rows), ss(1), rs(1))
-        send(buf(up, *hi_half), buf(up, *hi_half), ss(3), rs(3), (ep, down))
-        send(buf(up, *rows), buf(up, *rows), ss(6), rs(6), (ep, partner))
-
-    far, far_oc = yo * 2 + c, yo * 2 + oc
-    up_oc, down_oc = yp * 2 + oc, ym * 2 + oc
-
-    def gather_far(buf, half, ss, rs, rows):
-        first, size = rows
-        lo_half, hi_half = (first, half), (first + half, half)
-        arrive(buf(far, *lo_half), ss(2), rs(2))
-        send(buf(far, *lo_half), buf(far, *lo_half), ss(7), rs(7), (ep, partner))
-        arrive(buf(far, *hi_half), ss(3), rs(3))
-        send(buf(far, *hi_half), buf(far, *hi_half), ss(8), rs(8), (ep, partner))
-
-    def at1(t, first, size):
-        return g1.at[t, pl.ds(first, size), :]
-
-    one = (at1, ROWS // 2, lambda k: g1_s.at[k], lambda k: g1_r.at[k], (0, ROWS))
-    loads[0].wait()
-    pl.semaphore_wait(barrier, NTP + NEP - 2)
-    gather_send(*one)
     loads[1].wait()
     loads[2].wait()
 
@@ -211,8 +213,8 @@
         k_re, k_im = decay_re[g:g + 1, :], decay_im[g:g + 1, :]
         new_re = k_re * old_re - k_im * old_im + drive[:, (2 * g) * 128:(2 * g) * 128 + STATE]
         new_im = k_re * old_im + k_im * old_re + drive[:, (2 * g + 1) * 128:(2 * g + 1) * 128 + STATE]
-        new_state[pl.ds(g, ROWS, stride=2 * GRP), :] = new_re
-        new_state[pl.ds(GRP + g, ROWS, stride=2 * GRP), :] = new_im
+        state_out[pl.ds(g, ROWS, stride=2 * GRP), :] = new_re
+        state_out[pl.ds(GRP + g, ROWS, stride=2 * GRP), :] = new_im
         fresh[:, (2 * g) * 128:(2 * g) * 128 + STATE] = new_re.astype(BF)
         fresh[:, (2 * g + 1) * 128:(2 * g + 1) * 128 + STATE] = new_im.astype(BF)
     act = jax.nn.gelu(dot_nt(fresh[...], rbd[...]) + skip_row * u_in.astype(F32))
@@ -220,8 +222,6 @@
     act_all[tp] = act.astype(BF)
     for d in range(1, NTP):
         send(act_all.at[tp], act_all.at[tp], a_s.at[d], a_r.at[d], (ep, lax.rem(tp + d, NTP)))
-    store_state = pltpu.make_async_copy(new_state, state_out, st_sem)
-    store_state.start()
     loads[14].wait()
     loads[15].wait()
     for d in range(1, NTP):
@@ -245,9 +245,13 @@
         def sem(kind, i):
             return base + kind * sets + i
 
-        for j in range(4):
+        def to_partner(j):
             ds[j] = product(order[j] * 2 + oc).astype(BF)
             send(ds.at[j], dr.at[j], ss.at[j], rs.at[j], (ep, partner))
+
+        to_partner(0)
+        to_partner(1)
+        to_partner(2)
 
         def on_chip(j):
             value = product(order[j] * 2 + c)
@@ -258,6 +262,7 @@
         for i in range(sets):
             send(q.at[0, lo(i), :], rel.at[0, lo(i), :], ss.at[sem(0, i)], rs.at[sem(0, i)], (ep, up))
             send(q.at[0, hi(i), :], rel.at[1, lo(i), :], ss.at[sem(1, i)], rs.at[sem(1, i)], (ep, down))
+        to_partner(3)
         q[1] = on_chip(1).astype(BF)
 
         def direct_up(i):
@@ -373,27 +378,24 @@
                 arrive(at(t, first, half), ss(kinds[0]), rs(kinds[0]))
                 arrive(at(t, first + half, half), ss(kinds[1]), rs(kinds[1]))
 
-    start_chunk(0)
-    start_chunk(1)
+    for j in range(4):
+        start_chunk(j)
+    expert_block(tp)
     gather_relay(*plans[0])
-    start_chunk(2)
-    gather_relay(*plans[1])
-    gather_far(*plans[0])
-    start_chunk(3)
-    gather_relay(*plans[2])
-    gather_far(*plans[1])
-    expert_block(tp)
-    gather_relay(*plans[3])
     from_partner(partner, (4,))
     expert_block(partner)
-    gather_far(*plans[2])
+    for j in range(1, 4):
+        gather_relay(*plans[j])
     expert_block(down)
+    gather_far(*plans[0])
     expert_block(up)
-    gather_far(*plans[3])
+    gather_far(*plans[1])
     from_partner(down_oc, (5,))
     expert_block(down_oc)
+    gather_far(*plans[2])
     from_partner(up_oc, (6,))
     expert_block(up_oc)
+    gather_far(*plans[3])
     expert_block(far)
     from_partner(far_oc, (7, 8))
     expert_block(far_oc)
@@ -428,9 +430,7 @@
         e = lax.rem(ep + d, NEP)
         arrive(back.at[slot(e), :], ret_s.at[e], ret_r.at[e])
     combined = dot(wt[0], back[...]) + dot(wt[1], back[...])
-    v_layer[...] = (after[...].astype(F32) + combined).astype(BF)
-    finish = pltpu.make_async_copy(v_layer, out, load_sem.at[0])
-    finish.start()
+    out[...] = (after[...].astype(F32) + combined).astype(BF)
     for copy in sent:
         copy.wait_send()
     for d in range(1, NEP):
@@ -439,8 +439,14 @@
             src_ref=eout.at[slot(e), :], dst_ref=eout.at[slot(e), :], send_sem=ret_s.at[e], recv_sem=ret_r.at[e],
             device_id=(e, tp), device_id_type=MESH,
         ).wait_send()
-    store_state.wait()
-    finish.wait()
+
+
+def write_out(layer, state, layer_hbm, state_hbm, sems):
+    copies = [pltpu.make_async_copy(state, state_hbm, sems.at[0]), pltpu.make_async_copy(layer, layer_hbm, sems.at[1])]
+    for copy in copies:
+        copy.start()
+    for copy in copies:
+        copy.wait()
 
 
 def per_device(
@@ -466,7 +472,7 @@
     scratch = [vm(operands[i].shape, operands[i].dtype) for i in range(1, 20)]
     scratch += [
         vm((NTP, ROWS, WIDTH), BF), vm((128, 2048), BF), vm((128, 2048), BF),
-        vm((128, 2048), BF), vm((ROWS, 2048), BF), vm((ROWS * 2 * GRP, STATE), F32), vm((NTP, ROWS, 128), BF),
+        vm((128, 2048), BF), vm((ROWS, 2048), BF), vm((NTP, ROWS, 128), BF),
         vm((ROWS, 128), F32), vm((ROWS, 128), BF),
     ]
     scratch += exchange(ROWS)
@@ -476,26 +482,38 @@
         vm((SLOTS, FFW), BF),
     ]
     scratch += exchange(SLOTS)
-    scratch += [vm((SLOTS, WIDTH), BF), vm((SLOTS, WIDTH), BF), vm((ROWS, WIDTH), BF)]
+    scratch += [vm((SLOTS, WIDTH), BF), vm((SLOTS, WIDTH), BF)]
     scratch += [
         dma((20,)), dma((9,)), dma((9,)), dma((8,)), dma((8,)), dma((10,)), dma((10,)), dma((16,)), dma((16,)),
-        dma((4, 9)), dma((4, 9)), dma((16,)), dma((16,)), dma((16,)), dma((16,)), dma,
+        dma((4, 9)), dma((4, 9)), dma((16,)), dma((16,)), dma((16,)), dma((16,)),
     ]
-    anywhere = pl.BlockSpec(memory_space=pl.ANY)
+    anywhere = pl.BlockSpec(memory_space=pltpu.HBM)
+    outside = pl.BlockSpec(memory_space=pl.ANY)
+    inside = pl.BlockSpec(memory_space=pltpu.VMEM)
     layer_out, state_next = pl.pallas_call(
         kernel,
+        out_shape=(vm((ROWS, WIDTH), BF), vm((ROWS * 2 * GRP, STATE), F32)),
+        in_specs=[anywhere] * 20,
+        out_specs=(inside, inside),
+        scratch_shapes=scratch,
+        compiler_params=pltpu.CompilerParams(
+            collective_id=0, has_side_effects=True, vmem_limit_bytes=44 * 1024 * 1024
+        ),
+        name="layer",
+    )(*[pltpu.with_memory_space_constraint(a, pltpu.HBM) for a in operands])
+    layer_out = pltpu.with_memory_space_constraint(layer_out, pltpu.VMEM)
+    state_next = pltpu.with_memory_space_constraint(state_next, pltpu.VMEM)
+    layer_out, state_next = pl.pallas_call(
+        write_out,
         out_shape=(
             jax.ShapeDtypeStruct((ROWS, WIDTH), BF),
             jax.ShapeDtypeStruct((ROWS * 2 * GRP, STATE), F32),
         ),
-        in_specs=[anywhere] * 20,
-        out_specs=(anywhere, anywhere),
-        scratch_shapes=scratch,
-        compiler_params=pltpu.CompilerParams(
-            collective_id=0, has_side_effects=True, vmem_limit_bytes=60 * 1024 * 1024
-        ),
-        name="layer",
-    )(*operands)
+        in_specs=[inside] * 2,
+        out_specs=(outside, outside),
+        scratch_shapes=[dma((2,))],
+        name="write_out",
+    )(layer_out, state_next)
     return layer_out, state_next.reshape(ROWS, 2, GRP, STATE)
 
 

time: 74.4 us -> 65 us (0.87)
  Pallas kernels: 69.4 us -> 63.6 us
  local copies, waits for them, and re-layouts: 3.34 us -> 0 us
    pallas_call x1 -> x2, Pallas kernels: 69.4 us -> 63.6 us  [the longest x1 62.8 us: per_device(): pl.pallas_call(kernel, out_shape=(vm((ROWS, WIDTH), BF), vm((ROWS * 2 * G...]
    unnamed x2 -> x0, local copies, waits for them, and re-layouts: 3.34 us -> none
where the time goes in v2:
time: 65 us; the launch traced here: 64.3 us
  Pallas kernels  63.6 us (98%)
  between operations  0.65 us (1%)
    pallas_call x1, Pallas kernels, per_device(): pl.pallas_call(kernel, out_shape=(vm((ROWS, WIDTH), BF), vm((ROWS * 2 * G...  62.8 us

profile of v2, /device:TPU:0, one launch (start us, length us, event | category | flops | bytes accessed | tf_op | source)
XLA Modules:
  0.0 64.3 jit_solution(10725862484382542864)
XLA Ops:
  0.6 62.8 %layer.1 = (bf16[64,512]{1,0:T(8,128)(2,1)S(1)}, f32[1024,64]{1,0:T(8,128)S(1)}) custom-call(bf16[64,512]{1,0:T(8,128)(2,1)} %residual.1, s32[2,64]{1,0:T(2,128)} %bitcast.32, f32[2,64]{1,0:T(2,128)} %bitcast.33, f32[1024,64]{1,0:T(8,128)} %bitcast.25, f32[1,4096]{1,0:T(1,128)} %bitcast.30, f32[1,4096]{1,0:T(1,128)} %bitcast.31, bf16[4096,128]{1,0:T(8,128)(2,1)} %w_in.1, ...), custom_call_target="tpu_custom_call" | custom-call | tf_op jit(solution)/shard_map/layer/pallas_call | solution.py:493
  63.5 0.8 %write_out.1 = (bf16[64,512]{1,0:T(8,128)(2,1)}, f32[1024,64]{1,0:T(8,128)}) custom-call(bf16[64,512]{1,0:T(8,128)(2,1)S(1)} %get-tuple-element.6.layer, f32[1024,64]{1,0:T(8,128)S(1)} %get-tuple-element.7.state), custom_call_target="tpu_custom_call" | custom-call | tf_op jit(solution)/shard_map/write_out/pallas_call | solution.py:506

commit v3 on v2

v3 whole, which is shorter than its diff:
```python
import functools

import jax
import jax.numpy as jnp
from jax import lax
from jax.experimental import pallas as pl
from jax.experimental.pallas import tpu as pltpu
from jax.sharding import PartitionSpec as P

MESH = pl.DeviceIdType.MESH
BF = jnp.bfloat16
F32 = jnp.float32
EPS = 1e-06
NT = (((1,), (1,)), ((), ()))

NEP = 16
NTP = 8
ROWS = 64
WIDTH = 512
SLOT = 16
SLOTS = NEP * SLOT
FFW = 704
STATE = 64
GRP = 8
GCH = 16


def dot(a, b):
    return jnp.dot(a, b, preferred_element_type=F32)


def dot_nt(a, b):
    return lax.dot_general(a, b, NT, preferred_element_type=F32)


def iota(shape, dim):
    return lax.broadcasted_iota(jnp.int32, shape, dim)


def kernel(
    residual, routes, weights, state, mix_gain, ffn_gain, w_in, decay_rate, rotation,
    log_step, in_re, in_im, read_re, read_im, skip, w_glu, w_out, w_gate, w_up, w_down,
    out, state_out,
    v_routes, v_weights, v_state, v_gain, v_win, v_lam, v_step, v_io, v_skip, v_glu, v_out, v_gu, v_down,
    g1, bd_hi, bd_lo, rbd, fresh, act_all, act32, mixed,
    b_q, b_own, b_rel, b_dir, b_mrg, b_ms,
    v_glu2, wo2, after, d_map, wt, outb, g2, acc_g, acc_u, sq, hidden,
    e_ds, e_dr, e_q, e_own, e_rel, e_dir, e_mrg, e_ms, eout, back,
    load_sem, send_sem, g1_r, a_r, b_r, d_r, x_r, g2_r, e_r, ret_r,
):
    ep = lax.axis_index("ep")
    tp = lax.axis_index("tp")
    y, c = lax.div(tp, 2), lax.rem(tp, 2)
    z, x = lax.div(ep, 4), lax.rem(ep, 4)
    yp, ym, yo = lax.rem(y + 1, 4), lax.rem(y + 3, 4), lax.rem(y + 2, 4)
    oc = 1 - c
    partner = y * 2 + oc
    up, down = yp * 2 + c, ym * 2 + c
    def send(src, dst, exchange, rs, device):
        pltpu.make_async_remote_copy(
            src_ref=src, dst_ref=dst, send_sem=send_sem.at[exchange], recv_sem=rs, device_id=device, device_id_type=MESH
        ).start()

    def remote(ref, exchange, rs):
        return pltpu.make_async_remote_copy(
            src_ref=ref, dst_ref=ref, send_sem=send_sem.at[exchange], recv_sem=rs, device_id=(ep, partner),
            device_id_type=MESH,
        )

    def arrive(dst, rs):
        remote(dst, 0, rs).wait_recv()

    def left(ref, exchange):
        remote(ref, exchange, g1_r.at[0]).wait_send()

    groups = [
        [(residual, g1.at[tp])],
        [(w_in, v_win)],
        [(mix_gain, v_gain.at[0]), (ffn_gain, v_gain.at[1])],
        [(decay_rate, v_lam.at[0]), (rotation, v_lam.at[1])],
        [(log_step, v_step)],
        [(in_re, v_io.at[0]), (in_im, v_io.at[1]), (read_re, v_io.at[2]), (read_im, v_io.at[3])],
        [(skip, v_skip)],
        [(routes, v_routes)],
        [(weights, v_weights)],
        [(w_glu, v_glu)],
        [(w_out, v_out)],
        [(state, v_state)],
        [(w_gate, v_gu.at[0]), (w_up, v_gu.at[1])],
        [(w_down, v_down)],
    ]
    wholes = [
        g1.at[tp], v_win, v_gain, v_lam, v_step, v_io, v_skip, v_routes, v_weights, v_glu, v_out, v_state, v_gu, v_down
    ]

    def load(i):
        for src, dst in groups[i]:
            pltpu.make_async_copy(src, dst, load_sem.at[i]).start()

    def loaded(i):
        pltpu.make_async_copy(wholes[i], wholes[i], load_sem.at[i]).wait()

    load(0)

    barrier = pltpu.get_barrier_semaphore()
    for d in range(1, NTP):
        pl.semaphore_signal(barrier, inc=1, device_id=(ep, lax.rem(tp + d, NTP)), device_id_type=MESH)
    for d in range(1, NEP):
        pl.semaphore_signal(barrier, inc=1, device_id=(lax.rem(ep + d, NEP), tp), device_id_type=MESH)

    for i in range(1, len(groups)):
        load(i)

    order = (yo, yp, ym, y)

    def columns(t):
        return pl.ds(pl.multiple_of(t * WIDTH, WIDTH), WIDTH)

    def split_send(buf, half, rs, rows):
        first, size = rows
        lo_half, hi_half = (first, half), (first + half, half)
        send(buf(tp, *lo_half), buf(tp, *lo_half), 0, rs(0), (ep, up))
        send(buf(tp, *hi_half), buf(tp, *hi_half), 0, rs(1), (ep, down))
        send(buf(tp, *hi_half), buf(tp, *hi_half), 0, rs(2), (ep, up))
        send(buf(tp, *lo_half), buf(tp, *lo_half), 0, rs(3), (ep, down))
        send(buf(tp, *rows), buf(tp, *rows), 0, rs(4), (ep, partner))

    def split_relay(buf, half, rs, rows):
        first, size = rows
        lo_half, hi_half = (first, half), (first + half, half)
        arrive(buf(down, *lo_half), rs(0))
        send(buf(down, *lo_half), buf(down, *lo_half), 0, rs(5), (ep, up))
        arrive(buf(up, *hi_half), rs(1))
        send(buf(up, *hi_half), buf(up, *hi_half), 0, rs(5), (ep, down))
        arrive(buf(down, *hi_half), rs(2))
        send(buf(down, *rows), buf(down, *rows), 0, rs(6), (ep, partner))
        arrive(buf(up, *lo_half), rs(3))
        send(buf(up, *rows), buf(up, *rows), 0, rs(7), (ep, partner))

    far, far_oc = yo * 2 + c, yo * 2 + oc
    up_oc, down_oc = yp * 2 + oc, ym * 2 + oc

    def at1(t, first, size):
        return g1.at[t, pl.ds(first, size), :]

    one = (at1, ROWS // 2, lambda k: g1_r.at[k], (0, ROWS))
    loaded(0)
    pl.semaphore_wait(barrier, NTP + NEP - 2)
    split_send(*one)
    for i in range(3, 9):
        loaded(i)

    eye8 = iota((GRP, GRP), 0) == iota((GRP, GRP), 1)
    step = jnp.exp(jnp.sum(jnp.where(eye8, jnp.broadcast_to(v_step[...], (GRP, GRP)), 0.0), axis=1, keepdims=True))
    rate, rot = v_lam[0], v_lam[1]
    real = -rate
    magnitude = jnp.exp(real * step)
    angle = rot * step
    decay_re = magnitude * jnp.cos(angle)
    decay_im = magnitude * jnp.sin(angle)
    denominator = real * real + rot * rot
    lift_re = ((decay_re - 1.0) * real + decay_im * rot) / denominator
    lift_im = (decay_im * real - (decay_re - 1.0) * rot) / denominator
    bd_hi[...] = jnp.zeros_like(bd_hi)
    bd_lo[...] = jnp.zeros_like(bd_lo)
    rbd[...] = jnp.zeros_like(rbd)
    fresh[...] = jnp.zeros_like(fresh)
    for g in range(GRP):
        rows = slice(g * GCH, (g + 1) * GCH)
        l_re, l_im = lift_re[g:g + 1, :], lift_im[g:g + 1, :]
        b_re, b_im = v_io[0, rows, :], v_io[1, rows, :]
        for n, value in enumerate((l_re * b_re - l_im * b_im, l_re * b_im + l_im * b_re)):
            lanes = slice((2 * g + n) * 128, (2 * g + n) * 128 + STATE)
            hi = value.astype(BF)
            bd_hi[rows, lanes] = hi
            bd_lo[rows, lanes] = (value - hi.astype(F32)).astype(BF)
        rbd[rows, (2 * g) * 128:(2 * g) * 128 + STATE] = v_io[2, rows, :].astype(BF)
        rbd[rows, (2 * g + 1) * 128:(2 * g + 1) * 128 + STATE] = (-v_io[3, rows, :]).astype(BF)
    tiler = (iota((GCH, 128), 0) == lax.rem(iota((GCH, 128), 1), GCH)).astype(BF)
    skip_hi = v_skip[...].astype(BF)
    skip_rest = v_skip[...] - skip_hi.astype(F32)
    skip_mid = skip_rest.astype(BF)
    skip_lo = (skip_rest - skip_mid.astype(F32)).astype(BF)
    skip_rep = dot(skip_hi, tiler) + dot(skip_mid, tiler) + dot(skip_lo, tiler)
    skip_row = jnp.sum(
        jnp.where(lax.div(iota((GRP, 128), 1), GCH) == iota((GRP, 128), 0), skip_rep, 0.0), axis=0, keepdims=True
    )
    r0, r1 = v_routes[0:1, :], v_routes[1:2, :]
    oh0 = (r0 == iota((NEP, ROWS), 0)).astype(F32)
    oh1 = (r1 == iota((NEP, ROWS), 0)).astype(F32)
    upper_tri = (iota((ROWS, ROWS), 0) < iota((ROWS, ROWS), 1)).astype(BF)
    before = dot((oh0 + oh1).astype(BF), upper_tri)
    dest0 = r0.astype(F32) * SLOT + jnp.sum(before * oh0, axis=0, keepdims=True)
    dest1 = r1.astype(F32) * SLOT + jnp.sum(before * oh1, axis=0, keepdims=True)
    place = iota((SLOTS, ROWS), 0).astype(F32)
    m0, m1 = (dest0 == place).astype(F32), (dest1 == place).astype(F32)
    d_map[...] = (m0 + m1).astype(BF)
    w_all = jnp.transpose(v_weights[0:1, :] * m0 + v_weights[1:2, :] * m1)
    w_hi = w_all.astype(BF)
    wt[0] = w_hi
    wt[1] = (w_all - w_hi.astype(F32)).astype(BF)

    loaded(1)
    loaded(2)
    loaded(9)
    loaded(10)
    send(v_glu, v_glu2, 1, d_r.at[0], (ep, partner))
    for j in range(4):
        send(v_out.at[:, columns(order[j] * 2 + oc)], wo2.at[j], 2, d_r.at[1], (ep, partner))

    total = [None, None]

    def mix_block(t):
        rows = g1[t].astype(F32)
        squares = jnp.sum(rows * rows, axis=1, keepdims=True)
        gain = v_gain[0, :, columns(t)]
        product = dot((rows * gain).astype(BF), v_win[columns(t), :])
        total[0] = squares if total[0] is None else total[0] + squares
        total[1] = product if total[1] is None else total[1] + product

    mix_block(tp)
    split_relay(*one)
    mix_block(down)
    mix_block(up)
    arrive(g1.at[partner], g1_r.at[4])
    mix_block(partner)
    arrive(g1.at[far], g1_r.at[5])
    send(g1.at[far], g1.at[far], 0, g1_r.at[8], (ep, partner))
    arrive(g1.at[down_oc], g1_r.at[6])
    mix_block(down_oc)
    arrive(g1.at[up_oc], g1_r.at[7])
    mix_block(up_oc)
    mix_block(far)
    arrive(g1.at[far_oc], g1_r.at[8])
    mix_block(far_oc)
    u_in = (total[1] * lax.rsqrt(total[0] / (NTP * WIDTH) + EPS)).astype(BF)

    loaded(11)
    drive = dot(u_in, bd_hi[...]) + dot(u_in, bd_lo[...])
    for g in range(GRP):
        old_re = v_state[pl.ds(g, ROWS, stride=2 * GRP), :]
        old_im = v_state[pl.ds(GRP + g, ROWS, stride=2 * GRP), :]
        k_re, k_im = decay_re[g:g + 1, :], decay_im[g:g + 1, :]
        new_re = k_re * old_re - k_im * old_im + drive[:, (2 * g) * 128:(2 * g) * 128 + STATE]
        new_im = k_re * old_im + k_im * old_re + drive[:, (2 * g + 1) * 128:(2 * g + 1) * 128 + STATE]
        state_out[pl.ds(g, ROWS, stride=2 * GRP), :] = new_re
        state_out[pl.ds(GRP + g, ROWS, stride=2 * GRP), :] = new_im
        fresh[:, (2 * g) * 128:(2 * g) * 128 + STATE] = new_re.astype(BF)
        fresh[:, (2 * g + 1) * 128:(2 * g + 1) * 128 + STATE] = new_im.astype(BF)
    act = jax.nn.gelu(dot_nt(fresh[...], rbd[...]) + skip_row * u_in.astype(F32))
    act32[...] = act
    act_all[tp] = act.astype(BF)
    towards = (far, far_oc, up, down, up_oc, down_oc, partner)
    for t in towards:
        send(act_all.at[tp], act_all.at[tp], 3, a_r.at[0], (ep, t))
    arrive(v_glu2, d_r.at[0])
    arrive(wo2, d_r.at[1])
    arrive(act_all.at[0:NTP - 1], a_r.at[0])
    everything = jnp.concatenate([act_all[t] for t in range(NTP)], axis=1)
    mixed[0] = (act32[...] * jax.nn.sigmoid(dot(everything, v_glu[...]))).astype(BF)
    mixed[1] = (act_all[partner].astype(F32) * jax.nn.sigmoid(dot(everything, v_glu2[...]))).astype(BF)

    def scatter(q, rel, dire, mrg, ms, exchange, rs, base, piece, lo, hi):
        low, high = pl.ds(lo, piece), pl.ds(hi, piece)

        def far_blocks():
            send(q.at[0, low, :], rel.at[0], exchange, rs.at[base], (ep, up))
            send(q.at[0, high, :], rel.at[1], exchange, rs.at[base + 1], (ep, down))

        def near_up():
            send(q.at[1, high, :], dire.at[0], exchange, rs.at[base + 2], (ep, up))

        def near_down():
            send(q.at[2, low, :], dire.at[1], exchange, rs.at[base + 3], (ep, down))

        def merge():
            arrive(rel.at[0], rs.at[base])
            ms[0] = (q[1, lo:lo + piece, :].astype(F32) + rel[0].astype(F32)).astype(BF)
            send(ms.at[0], mrg.at[0], exchange, rs.at[base + 4], (ep, up))
            arrive(rel.at[1], rs.at[base + 1])
            ms[1] = (q[2, hi:hi + piece, :].astype(F32) + rel[1].astype(F32)).astype(BF)
            send(ms.at[1], mrg.at[1], exchange, rs.at[base + 5], (ep, down))

        def final(own, done):
            arrive(dire.at[1], rs.at[base + 3])
            arrive(mrg.at[0], rs.at[base + 4])
            done(0, own[lo:lo + piece, :] + dire[1].astype(F32) + mrg[0].astype(F32))
            arrive(dire.at[0], rs.at[base + 2])
            arrive(mrg.at[1], rs.at[base + 5])
            done(1, own[hi:hi + piece, :] + dire[0].astype(F32) + mrg[1].astype(F32))

        return far_blocks, near_up, near_down, merge, final

    def branch_done(part, value):
        rows = slice(part * (ROWS // 2), (part + 1) * (ROWS // 2))
        after[rows, :] = (g1[tp, rows, :].astype(F32) + value).astype(BF)

    def chip_product(j):
        return dot(mixed[0], v_out[:, columns(order[j] * 2 + c)]) + dot(mixed[1], wo2[j])

    far_blocks, near_up, near_down, merge, final = scatter(
        b_q, b_rel, b_dir, b_mrg, b_ms, 4, b_r, 0, ROWS // 2, 0, ROWS // 2
    )
    b_q[0] = chip_product(0).astype(BF)
    far_blocks()
    b_q[1] = chip_product(1).astype(BF)
    near_up()
    b_q[2] = chip_product(2).astype(BF)
    near_down()
    b_own[...] = chip_product(3)
    merge()
    final(b_own, branch_done)

    outb[...] = dot(d_map[...], after[...]).astype(BF)

    def slot(e):
        return pl.ds(pl.multiple_of(e * SLOT, SLOT), SLOT)

    turns = (2, 3, 1, 0)
    chunk = SLOTS // 4
    across = (2, 1, 3, 0)

    def spot(j, xx):
        return pl.ds(pl.multiple_of(j * chunk + xx * SLOT, SLOT), SLOT)

    def rows_of(j):
        return pl.ds(j * chunk, chunk)

    for j in (3, 2, 1, 0):
        dz = turns[j]
        for dx in across:
            if (dz, dx) != (0, 0):
                e = lax.rem(z + dz, 4) * 4 + lax.rem(x + dx, 4)
                send(outb.at[slot(e), :], g2.at[tp, spot(j, x), :], 5, x_r.at[j], (e, tp))
    g2[tp, spot(3, x), :] = outb[slot(ep), :]
    loaded(12)

    def start_chunk(j):
        arrive(g2.at[tp, pl.ds(j * chunk, chunk if turns[j] else chunk - SLOT), :], x_r.at[j])
        block = g2.at[tp, rows_of(j), :]
        send(block, block, 6, g2_r.at[j], (ep, up))
        send(block, block, 6, g2_r.at[4 + j], (ep, down))
        send(block, block, 6, g2_r.at[12], (ep, partner))

    def relay(j):
        first = g2.at[down, rows_of(j), :]
        arrive(first, g2_r.at[j])
        low = g2.at[down, pl.ds(j * chunk, chunk // 2), :]
        send(low, low, 6, g2_r.at[8 + j], (ep, up))
        send(first, first, 6, g2_r.at[13], (ep, partner))
        second = g2.at[up, rows_of(j), :]
        arrive(second, g2_r.at[4 + j])
        high = g2.at[up, pl.ds(j * chunk + chunk // 2, chunk // 2), :]
        send(high, high, 6, g2_r.at[8 + j], (ep, down))
        send(second, second, 6, g2_r.at[14], (ep, partner))

    def pass_far(j):
        block = g2.at[far, rows_of(j), :]
        arrive(block, g2_r.at[8 + j])
        send(block, block, 6, g2_r.at[15], (ep, partner))

    def expert_block(t, first=False):
        rows = g2[t].astype(F32)
        scaled = (rows * v_gain[1, :, columns(t)]).astype(BF)
        squares = rows * rows
        squares = squares[:, 0:128] + squares[:, 128:256] + squares[:, 256:384] + squares[:, 384:512]
        gate, upper = dot_nt(scaled, v_gu[0, :, columns(t)]), dot_nt(scaled, v_gu[1, :, columns(t)])
        if first:
            sq[...] = squares
            acc_g[...] = gate
            acc_u[...] = upper
        else:
            sq[...] += squares
            acc_g[...] += gate
            acc_u[...] += upper

    def from_partner(t, k):
        arrive(g2.at[t], g2_r.at[k])
        expert_block(t)

    for j in (3, 2, 1, 0):
        start_chunk(j)
    expert_block(tp, True)
    relay(3)
    from_partner(partner, 12)
    relay(2)
    relay(1)
    relay(0)
    expert_block(down)
    pass_far(3)
    expert_block(up)
    pass_far(2)
    from_partner(down_oc, 13)
    pass_far(1)
    from_partner(up_oc, 14)
    pass_far(0)
    expert_block(far)
    from_partner(far_oc, 15)

    for r in range(0, SLOTS, 64):
        scale = lax.rsqrt(jnp.sum(sq[r:r + 64, :], axis=1, keepdims=True) / (NTP * WIDTH) + EPS)
        gate, upper = acc_g[r:r + 64, :] * scale, acc_u[r:r + 64, :] * scale
        hidden[r:r + 64, :] = (gate * jax.nn.sigmoid(gate) * upper).astype(BF)
    loaded(13)

    def product(t):
        return dot(hidden[...], v_down[:, columns(t)])

    def to_partner(j):
        e_ds[j] = product(order[j] * 2 + oc).astype(BF)
        send(e_ds.at[j], e_dr.at[j], 7, e_r.at[j], (ep, partner))

    def on_chip(j):
        value = product(order[j] * 2 + c)
        arrive(e_dr.at[j], e_r.at[j])
        return value + e_dr[j].astype(F32)

    def expert_done(i):
        def done(part, value):
            j = 2 * part + i
            eout[j * chunk:(j + 1) * chunk, :] = value.astype(BF)
            dz = turns[j]
            for dx in across:
                from_x = lax.rem(x + 4 - dx, 4)
                here = spot(j, from_x)
                if dz or dx:
                    s = lax.rem(z + 4 - dz, 4) * 4 + from_x
                    send(eout.at[here, :], back.at[slot(ep), :], 9, ret_r.at[0], (s, tp))
                else:
                    back[slot(ep), :] = eout[here, :]
        return done

    stages = [
        scatter(
            e_q, e_rel.at[i], e_dir.at[i], e_mrg.at[i], e_ms.at[i], 8, e_r, 4 + 6 * i, chunk, i * chunk, (2 + i) * chunk
        )
        for i in range(2)
    ]
    to_partner(0)
    to_partner(1)
    to_partner(2)
    e_q[0] = on_chip(0).astype(BF)
    stages[0][0]()
    stages[1][0]()
    to_partner(3)
    e_q[1] = on_chip(1).astype(BF)
    stages[0][1]()
    e_q[2] = on_chip(2).astype(BF)
    stages[0][2]()
    e_own[...] = on_chip(3)
    stages[0][3]()
    stages[1][1]()
    stages[1][2]()
    stages[1][3]()
    stages[0][4](e_own, expert_done(0))
    stages[1][4](e_own, expert_done(1))
    arrive(back.at[0:SLOTS - SLOT, :], ret_r.at[0])
    combined = dot(wt[0], back[...]) + dot(wt[1], back[...])
    out[...] = (after[...].astype(F32) + combined).astype(BF)
    left(g1.at[0:NTP - 1], 0)
    left(v_glu, 1)
    left(wo2, 2)
    left(act_all.at[0:NTP - 1], 3)
    left(b_q, 4)
    left(outb.at[0:SLOTS - SLOT, :], 5)
    left(g2.at[0:NTP - 1], 6)
    left(e_ds, 7)
    left(e_q, 8)
    left(eout.at[0:SLOTS - SLOT, :], 9)


def write_out(layer, state, layer_hbm, state_hbm, sems):
    copies = [pltpu.make_async_copy(state, state_hbm, sems.at[0]), pltpu.make_async_copy(layer, layer_hbm, sems.at[1])]
    for copy in copies:
        copy.start()
    for copy in copies:
        copy.wait()


def per_device(
    residual, routes, route_weights, state_prev, mix_gain, ffn_gain, w_in, decay_rate, rotation,
    log_step, in_re, in_im, read_re, read_im, skip_gain, w_glu, w_out, w_gate, w_up, w_down,
):
    dma = pltpu.SemaphoreType.DMA
    vm = pltpu.VMEM
    operands = (
        residual, routes.T, route_weights.T, state_prev.reshape(ROWS * 2 * GRP, STATE), mix_gain.reshape(1, -1),
        ffn_gain.reshape(1, -1), w_in, decay_rate, rotation, log_step.reshape(1, GRP),
        in_re.transpose(0, 2, 1).reshape(GRP * GCH, STATE), in_im.transpose(0, 2, 1).reshape(GRP * GCH, STATE), read_re.reshape(GRP * GCH, STATE),
        read_im.reshape(GRP * GCH, STATE), skip_gain, w_glu, w_out, w_gate[0].T, w_up[0].T, w_down[0],
    )

    def exchange(lead, rows, part):
        return [vm((3, rows, WIDTH), BF), vm((rows, WIDTH), F32)] + [vm((*lead, 2, part, WIDTH), BF)] * 4

    scratch = [
        vm((2, ROWS), jnp.int32), vm((2, ROWS), F32), vm((ROWS * 2 * GRP, STATE), F32), vm((2, 1, NTP * WIDTH), F32),
        vm((NTP * WIDTH, 128), BF), vm((2, GRP, STATE), F32), vm((1, GRP), F32), vm((4, GRP * GCH, STATE), F32),
        vm((GRP, GCH), F32), vm((NEP * ROWS, 128), BF), vm((128, NTP * WIDTH), BF), vm((2, FFW, NTP * WIDTH), BF),
        vm((FFW, NTP * WIDTH), BF),
    ]
    scratch += [
        vm((NTP, ROWS, WIDTH), BF), vm((128, 2048), BF), vm((128, 2048), BF),
        vm((128, 2048), BF), vm((ROWS, 2048), BF), vm((NTP, ROWS, 128), BF),
        vm((ROWS, 128), F32), vm((2, ROWS, 128), BF),
    ]
    scratch += exchange((), ROWS, ROWS // 2)
    scratch += [
        vm((NEP * ROWS, 128), BF), vm((4, 128, WIDTH), BF),
        vm((ROWS, WIDTH), BF), vm((SLOTS, ROWS), BF), vm((2, ROWS, SLOTS), BF), vm((SLOTS, WIDTH), BF),
        vm((NTP, SLOTS, WIDTH), BF), vm((SLOTS, FFW), F32), vm((SLOTS, FFW), F32), vm((SLOTS, 128), F32),
        vm((SLOTS, FFW), BF),
    ]
    scratch += [vm((4, SLOTS, WIDTH), BF)] * 2 + exchange((2,), SLOTS, SLOTS // 4)
    scratch += [vm((SLOTS, WIDTH), BF), vm((SLOTS, WIDTH), BF)]
    scratch += [
        dma((14,)), dma((10,)), dma((9,)), dma((1,)), dma((6,)), dma((2,)), dma((4,)), dma((16,)), dma((16,)), dma((1,))
    ]
    anywhere = pl.BlockSpec(memory_space=pltpu.HBM)
    outside = pl.BlockSpec(memory_space=pl.ANY)
    inside = pl.BlockSpec(memory_space=pltpu.VMEM)
    layer_out, state_next = pl.pallas_call(
        kernel,
        out_shape=(vm((ROWS, WIDTH), BF), vm((ROWS * 2 * GRP, STATE), F32)),
        in_specs=[anywhere] * 20,
        out_specs=(inside, inside),
        scratch_shapes=scratch,
        compiler_params=pltpu.CompilerParams(
            collective_id=0, has_side_effects=True, vmem_limit_bytes=44 * 1024 * 1024
        ),
        name="layer",
    )(*[pltpu.with_memory_space_constraint(a, pltpu.HBM) for a in operands])
    layer_out = pltpu.with_memory_space_constraint(layer_out, pltpu.VMEM)
    state_next = pltpu.with_memory_space_constraint(state_next, pltpu.VMEM)
    layer_out, state_next = pl.pallas_call(
        write_out,
        out_shape=(
            jax.ShapeDtypeStruct((ROWS, WIDTH), BF),
            jax.ShapeDtypeStruct((ROWS * 2 * GRP, STATE), F32),
        ),
        in_specs=[inside] * 2,
        out_specs=(outside, outside),
        scratch_shapes=[dma((2,))],
        name="write_out",
    )(layer_out, state_next)
    return layer_out, state_next.reshape(ROWS, 2, GRP, STATE)


def solution(mesh):
    return jax.shard_map(
        per_device,
        mesh=mesh,
        in_specs=(
            P("ep", "tp"), P("ep", None), P("ep", None), P("ep", None, "tp", None), P(), P(), P(None, "tp"),
            P("tp", None), P("tp", None), P("tp"), P("tp", None, None), P("tp", None, None), P("tp", None, None),
            P("tp", None, None), P("tp", None), P(None, "tp"), P("tp", None), P("ep", None, "tp"),
            P("ep", None, "tp"), P("ep", "tp", None),
        ),
        out_specs=(P("ep", "tp"), P("ep", None, "tp", None)),
        check_vma=False,
    )
```

time: 65 us -> 63.1 us (0.971); the launches traced: 64.3 us -> 63 us
  Pallas kernels: 63.6 us -> 62.4 us
    pallas_call x1, Pallas kernels: 62.8 us -> 61.6 us  [per_device(): pl.pallas_call(kernel, out_shape=(vm((ROWS, WIDTH), BF), vm((ROWS * 2 * G...]
where the time goes in v3:
time: 63.1 us; the launch traced here: 63 us
  Pallas kernels  62.4 us (99%)
  between operations  0.65 us (1%)
    pallas_call x1, Pallas kernels, per_device(): pl.pallas_call(kernel, out_shape=(vm((ROWS, WIDTH), BF), vm((ROWS * 2 * G...  61.6 us

profile of v3, /device:TPU:0, one launch (start us, length us, event | category | flops | bytes accessed | tf_op | source)
XLA Modules:
  0.0 63.0 jit_solution(18021390773014572475)
XLA Ops:
  0.6 61.6 %layer.1 = (bf16[64,512]{1,0:T(8,128)(2,1)S(1)}, f32[1024,64]{1,0:T(8,128)S(1)}) custom-call(bf16[64,512]{1,0:T(8,128)(2,1)} %residual.1, s32[2,64]{1,0:T(2,128)} %bitcast.32, f32[2,64]{1,0:T(2,128)} %bitcast.33, f32[1024,64]{1,0:T(8,128)} %bitcast.25, f32[1,4096]{1,0:T(1,128)} %bitcast.30, f32[1,4096]{1,0:T(1,128)} %bitcast.31, bf16[4096,128]{1,0:T(8,128)(2,1)} %w_in.1, ...), custom_call_target="tpu_custom_call" | custom-call | tf_op jit(solution)/shard_map/layer/pallas_call | solution.py:522
  62.2 0.8 %write_out.1 = (bf16[64,512]{1,0:T(8,128)(2,1)}, f32[1024,64]{1,0:T(8,128)}) custom-call(bf16[64,512]{1,0:T(8,128)(2,1)S(1)} %get-tuple-element.6.layer, f32[1024,64]{1,0:T(8,128)S(1)} %get-tuple-element.7.state), custom_call_target="tpu_custom_call" | custom-call | tf_op jit(solution)/shard_map/write_out/pallas_call | solution.py:535

commit v4 on v3

--- a/solution.py
+++ b/solution.py
@@ -42,7 +42,7 @@
     log_step, in_re, in_im, read_re, read_im, skip, w_glu, w_out, w_gate, w_up, w_down,
     out, state_out,
     v_routes, v_weights, v_state, v_gain, v_win, v_lam, v_step, v_io, v_skip, v_glu, v_out, v_gu, v_down,
-    g1, bd_hi, bd_lo, rbd, fresh, act_all, act32, mixed,
+    g1, thru, bd_hi, bd_lo, rbd, fresh, act_all, act32, mixed,
     b_q, b_own, b_rel, b_dir, b_mrg, b_ms,
     v_glu2, wo2, after, d_map, wt, outb, g2, acc_g, acc_u, sq, hidden,
     e_ds, e_dr, e_q, e_own, e_rel, e_dir, e_mrg, e_ms, eout, back,
@@ -130,8 +130,10 @@
         lo_half, hi_half = (first, half), (first + half, half)
         arrive(buf(down, *lo_half), rs(0))
         send(buf(down, *lo_half), buf(down, *lo_half), 0, rs(5), (ep, up))
+        send(buf(down, *lo_half), buf(down, *lo_half), 0, rs(8), (ep, up_oc))
         arrive(buf(up, *hi_half), rs(1))
         send(buf(up, *hi_half), buf(up, *hi_half), 0, rs(5), (ep, down))
+        send(buf(up, *hi_half), buf(up, *hi_half), 0, rs(8), (ep, down_oc))
         arrive(buf(down, *hi_half), rs(2))
         send(buf(down, *rows), buf(down, *rows), 0, rs(6), (ep, partner))
         arrive(buf(up, *lo_half), rs(3))
@@ -176,6 +178,21 @@
             bd_lo[rows, lanes] = (value - hi.astype(F32)).astype(BF)
         rbd[rows, (2 * g) * 128:(2 * g) * 128 + STATE] = v_io[2, rows, :].astype(BF)
         rbd[rows, (2 * g + 1) * 128:(2 * g + 1) * 128 + STATE] = (-v_io[3, rows, :]).astype(BF)
+    loaded(11)
+    for g in range(GRP):
+        old_re = v_state[pl.ds(g, ROWS, stride=2 * GRP), :]
+        old_im = v_state[pl.ds(GRP + g, ROWS, stride=2 * GRP), :]
+        k_re, k_im = decay_re[g:g + 1, :], decay_im[g:g + 1, :]
+        kept_re, kept_im = k_re * old_re - k_im * old_im, k_re * old_im + k_im * old_re
+        state_out[pl.ds(g, ROWS, stride=2 * GRP), :] = kept_re
+        state_out[pl.ds(GRP + g, ROWS, stride=2 * GRP), :] = kept_im
+        fresh[:, (2 * g) * 128:(2 * g) * 128 + STATE] = kept_re.astype(BF)
+        fresh[:, (2 * g + 1) * 128:(2 * g + 1) * 128 + STATE] = kept_im.astype(BF)
+    act32[...] = dot_nt(fresh[...], rbd[...])
+    through = dot_nt(bd_hi[...], rbd[...]) + dot_nt(bd_lo[...], rbd[...])
+    through_hi = through.astype(BF)
+    thru[0] = through_hi
+    thru[1] = (through - through_hi.astype(F32)).astype(BF)
     tiler = (iota((GCH, 128), 0) == lax.rem(iota((GCH, 128), 1), GCH)).astype(BF)
     skip_hi = v_skip[...].astype(BF)
     skip_rest = v_skip[...] - skip_hi.astype(F32)
@@ -224,35 +241,26 @@
     mix_block(up)
     arrive(g1.at[partner], g1_r.at[4])
     mix_block(partner)
-    arrive(g1.at[far], g1_r.at[5])
-    send(g1.at[far], g1.at[far], 0, g1_r.at[8], (ep, partner))
     arrive(g1.at[down_oc], g1_r.at[6])
     mix_block(down_oc)
     arrive(g1.at[up_oc], g1_r.at[7])
     mix_block(up_oc)
+    arrive(g1.at[far], g1_r.at[5])
     mix_block(far)
     arrive(g1.at[far_oc], g1_r.at[8])
     mix_block(far_oc)
     u_in = (total[1] * lax.rsqrt(total[0] / (NTP * WIDTH) + EPS)).astype(BF)
 
-    loaded(11)
-    drive = dot(u_in, bd_hi[...]) + dot(u_in, bd_lo[...])
-    for g in range(GRP):
-        old_re = v_state[pl.ds(g, ROWS, stride=2 * GRP), :]
-        old_im = v_state[pl.ds(GRP + g, ROWS, stride=2 * GRP), :]
-        k_re, k_im = decay_re[g:g + 1, :], decay_im[g:g + 1, :]
-        new_re = k_re * old_re - k_im * old_im + drive[:, (2 * g) * 128:(2 * g) * 128 + STATE]
-        new_im = k_re * old_im + k_im * old_re + drive[:, (2 * g + 1) * 128:(2 * g + 1) * 128 + STATE]
-        state_out[pl.ds(g, ROWS, stride=2 * GRP), :] = new_re
-        state_out[pl.ds(GRP + g, ROWS, stride=2 * GRP), :] = new_im
-        fresh[:, (2 * g) * 128:(2 * g) * 128 + STATE] = new_re.astype(BF)
-        fresh[:, (2 * g + 1) * 128:(2 * g + 1) * 128 + STATE] = new_im.astype(BF)
-    act = jax.nn.gelu(dot_nt(fresh[...], rbd[...]) + skip_row * u_in.astype(F32))
+    act = jax.nn.gelu(act32[...] + dot(u_in, thru[0]) + dot(u_in, thru[1]) + skip_row * u_in.astype(F32))
     act32[...] = act
     act_all[tp] = act.astype(BF)
     towards = (far, far_oc, up, down, up_oc, down_oc, partner)
     for t in towards:
         send(act_all.at[tp], act_all.at[tp], 3, a_r.at[0], (ep, t))
+    drive = dot(u_in, bd_hi[...]) + dot(u_in, bd_lo[...])
+    for g in range(GRP):
+        state_out[pl.ds(g, ROWS, stride=2 * GRP), :] += drive[:, (2 * g) * 128:(2 * g) * 128 + STATE]
+        state_out[pl.ds(GRP + g, ROWS, stride=2 * GRP), :] += drive[:, (2 * g + 1) * 128:(2 * g + 1) * 128 + STATE]
     arrive(v_glu2, d_r.at[0])
     arrive(wo2, d_r.at[1])
     arrive(act_all.at[0:NTP - 1], a_r.at[0])
@@ -316,27 +324,27 @@
     def slot(e):
         return pl.ds(pl.multiple_of(e * SLOT, SLOT), SLOT)
 
-    turns = (2, 3, 1, 0)
     chunk = SLOTS // 4
-    across = (2, 1, 3, 0)
-
-    def spot(j, xx):
-        return pl.ds(pl.multiple_of(j * chunk + xx * SLOT, SLOT), SLOT)
+    turns = (
+        ((2, 2), (2, 1), (2, 3), (3, 2)), ((1, 2), (3, 3), (3, 1), (1, 3)),
+        ((1, 1), (2, 0), (0, 2), (3, 0)), ((1, 0), (0, 3), (0, 1), (0, 0)),
+    )
 
     def rows_of(j):
         return pl.ds(j * chunk, chunk)
 
     for j in (3, 2, 1, 0):
-        dz = turns[j]
-        for dx in across:
-            if (dz, dx) != (0, 0):
+        for m, (dz, dx) in enumerate(turns[j]):
+            here = slice(j * chunk + m * SLOT, j * chunk + (m + 1) * SLOT)
+            if dz or dx:
                 e = lax.rem(z + dz, 4) * 4 + lax.rem(x + dx, 4)
-                send(outb.at[slot(e), :], g2.at[tp, spot(j, x), :], 5, x_r.at[j], (e, tp))
-    g2[tp, spot(3, x), :] = outb[slot(ep), :]
+                send(outb.at[slot(e), :], g2.at[tp, here, :], 5, x_r.at[j], (e, tp))
+            else:
+                g2[tp, here, :] = outb[slot(ep), :]
     loaded(12)
 
     def start_chunk(j):
-        arrive(g2.at[tp, pl.ds(j * chunk, chunk if turns[j] else chunk - SLOT), :], x_r.at[j])
+        arrive(g2.at[tp, pl.ds(j * chunk, chunk if j < 3 else chunk - SLOT), :], x_r.at[j])
         block = g2.at[tp, rows_of(j), :]
         send(block, block, 6, g2_r.at[j], (ep, up))
         send(block, block, 6, g2_r.at[4 + j], (ep, down))
@@ -382,8 +390,8 @@
         start_chunk(j)
     expert_block(tp, True)
     relay(3)
+    relay(2)
     from_partner(partner, 12)
-    relay(2)
     relay(1)
     relay(0)
     expert_block(down)
@@ -397,11 +405,22 @@
     expert_block(far)
     from_partner(far_oc, 15)
 
-    for r in range(0, SLOTS, 64):
-        scale = lax.rsqrt(jnp.sum(sq[r:r + 64, :], axis=1, keepdims=True) / (NTP * WIDTH) + EPS)
-        gate, upper = acc_g[r:r + 64, :] * scale, acc_u[r:r + 64, :] * scale
-        hidden[r:r + 64, :] = (gate * jax.nn.sigmoid(gate) * upper).astype(BF)
-    loaded(13)
+    def activate(i):
+        for r in (2 * i * chunk, (2 * i + 1) * chunk):
+            scale = lax.rsqrt(jnp.sum(sq[r:r + 64, :], axis=1, keepdims=True) / (NTP * WIDTH) + EPS)
+            gate, upper = acc_g[r:r + 64, :] * scale, acc_u[r:r + 64, :] * scale
+            hidden[r:r + 64, :] = (gate * jax.nn.sigmoid(gate) * upper).astype(BF)
+
+    def far_partner(i):
+        rows = slice(2 * i * chunk, 2 * (i + 1) * chunk)
+        e_ds[0, rows, :] = dot(hidden[rows, :], v_down[:, columns(far_oc)]).astype(BF)
+        send(e_ds.at[0, rows, :], e_dr.at[0, rows, :], 7, e_r.at[16 * i], (ep, partner))
+
+    def far_chip(i):
+        rows = slice(2 * i * chunk, 2 * (i + 1) * chunk)
+        value = dot(hidden[rows, :], v_down[:, columns(far)])
+        arrive(e_dr.at[0, rows, :], e_r.at[16 * i])
+        e_q[0, rows, :] = (value + e_dr[0, rows, :].astype(F32)).astype(BF)
 
     def product(t):
         return dot(hidden[...], v_down[:, columns(t)])
@@ -417,14 +436,12 @@
 
     def expert_done(i):
         def done(part, value):
-            j = 2 * part + i
+            j = 2 * i + part
             eout[j * chunk:(j + 1) * chunk, :] = value.astype(BF)
-            dz = turns[j]
-            for dx in across:
-                from_x = lax.rem(x + 4 - dx, 4)
-                here = spot(j, from_x)
+            for m, (dz, dx) in enumerate(turns[j]):
+                here = slice(j * chunk + m * SLOT, j * chunk + (m + 1) * SLOT)
                 if dz or dx:
-                    s = lax.rem(z + 4 - dz, 4) * 4 + from_x
+                    s = lax.rem(z + 4 - dz, 4) * 4 + lax.rem(x + 4 - dx, 4)
                     send(eout.at[here, :], back.at[slot(ep), :], 9, ret_r.at[0], (s, tp))
                 else:
                     back[slot(ep), :] = eout[here, :]
@@ -432,16 +449,21 @@
 
     stages = [
         scatter(
-            e_q, e_rel.at[i], e_dir.at[i], e_mrg.at[i], e_ms.at[i], 8, e_r, 4 + 6 * i, chunk, i * chunk, (2 + i) * chunk
+            e_q, e_rel.at[i], e_dir.at[i], e_mrg.at[i], e_ms.at[i], 8, e_r, 4 + 6 * i, chunk, 2 * i * chunk, (2 * i + 1) * chunk
         )
         for i in range(2)
     ]
-    to_partner(0)
+    activate(0)
+    loaded(13)
+    far_partner(0)
+    activate(1)
+    far_partner(1)
     to_partner(1)
+    far_chip(0)
+    stages[0][0]()
+    far_chip(1)
+    stages[1][0]()
     to_partner(2)
-    e_q[0] = on_chip(0).astype(BF)
-    stages[0][0]()
-    stages[1][0]()
     to_partner(3)
     e_q[1] = on_chip(1).astype(BF)
     stages[0][1]()
@@ -500,7 +522,7 @@
         vm((FFW, NTP * WIDTH), BF),
     ]
     scratch += [
-        vm((NTP, ROWS, WIDTH), BF), vm((128, 2048), BF), vm((128, 2048), BF),
+        vm((NTP, ROWS, WIDTH), BF), vm((2, 128, 128), BF), vm((128, 2048), BF), vm((128, 2048), BF),
         vm((128, 2048), BF), vm((ROWS, 2048), BF), vm((NTP, ROWS, 128), BF),
         vm((ROWS, 128), F32), vm((2, ROWS, 128), BF),
     ]
@@ -514,7 +536,7 @@
     scratch += [vm((4, SLOTS, WIDTH), BF)] * 2 + exchange((2,), SLOTS, SLOTS // 4)
     scratch += [vm((SLOTS, WIDTH), BF), vm((SLOTS, WIDTH), BF)]
     scratch += [
-        dma((14,)), dma((10,)), dma((9,)), dma((1,)), dma((6,)), dma((2,)), dma((4,)), dma((16,)), dma((16,)), dma((1,))
+        dma((14,)), dma((10,)), dma((9,)), dma((1,)), dma((6,)), dma((2,)), dma((4,)), dma((16,)), dma((17,)), dma((1,))
     ]
     anywhere = pl.BlockSpec(memory_space=pltpu.HBM)
     outside = pl.BlockSpec(memory_space=pl.ANY)

time: 63.1 us -> 59.9 us (0.949)
  Pallas kernels: 62.4 us -> 59.2 us
    pallas_call x1, Pallas kernels: 61.6 us -> 58.3 us  [per_device(): pl.pallas_call(kernel, out_shape=(vm((ROWS, WIDTH), BF), vm((ROWS * 2 * G...]
where the time goes in v4:
time: 59.9 us; the launch traced here: 59.8 us
  Pallas kernels  59.2 us (99%)
  between operations  0.65 us (1%)
    pallas_call x1, Pallas kernels, per_device(): pl.pallas_call(kernel, out_shape=(vm((ROWS, WIDTH), BF), vm((ROWS * 2 * G...  58.3 us

profile of v4, /device:TPU:0, one launch (start us, length us, event | category | flops | bytes accessed | tf_op | source)
XLA Modules:
  0.0 59.8 jit_solution(2445591712727980031)
XLA Ops:
  0.6 58.3 %layer.1 = (bf16[64,512]{1,0:T(8,128)(2,1)S(1)}, f32[1024,64]{1,0:T(8,128)S(1)}) custom-call(bf16[64,512]{1,0:T(8,128)(2,1)} %residual.1, s32[2,64]{1,0:T(2,128)} %bitcast.32, f32[2,64]{1,0:T(2,128)} %bitcast.33, f32[1024,64]{1,0:T(8,128)} %bitcast.25, f32[1,4096]{1,0:T(1,128)} %bitcast.30, f32[1,4096]{1,0:T(1,128)} %bitcast.31, bf16[4096,128]{1,0:T(8,128)(2,1)} %w_in.1, ...), custom_call_target="tpu_custom_call" | custom-call | tf_op jit(solution)/shard_map/layer/pallas_call | solution.py:544
  59.0 0.8 %write_out.1 = (bf16[64,512]{1,0:T(8,128)(2,1)}, f32[1024,64]{1,0:T(8,128)}) custom-call(bf16[64,512]{1,0:T(8,128)(2,1)S(1)} %get-tuple-element.6.layer, f32[1024,64]{1,0:T(8,128)S(1)} %get-tuple-element.7.state), custom_call_target="tpu_custom_call" | custom-call | tf_op jit(solution)/shard_map/write_out/pallas_call | solution.py:557
